TPU v7x, 128 devices: a whole 4x4x4 slice. The times are simulated.
128 devices in a mesh: ep: 32 (over z, y, core), tp: 4 (over x).
Axes of the slice: x: 4, y: 4, z: 4, core: 2. Of those that a mesh axis runs over, the one named last changes fastest.
Arguments:
- tokens: bfloat16 [1024, 2048], P('ep'), may hold values from -6 to 6
- kv_cache: bfloat16 [1024, 1024, 512], P('ep', None, 'tp'), may hold values from -320 to 320
- lengths: int32 [1024], P('ep'), may hold values from 1 to 1024, 524288 in all
- attn_gain: float32 [2048], replicated, may hold values from 0.1 to 1.9
- w_query: bfloat16 [2048, 1024], P(None, 'tp'), may hold values from -0.125 to 0.125
- w_key: bfloat16 [2048, 256], P(None, 'tp'), may hold values from -0.125 to 0.125
- w_value: bfloat16 [2048, 256], P(None, 'tp'), may hold values from -0.125 to 0.125
- lambdas: float32 [16], P('tp'), may hold values from 0.3 to 0.8
- head_gain: float32 [64], replicated, may hold values from 0.1 to 1.9
- w_out: bfloat16 [1024, 2048], replicated, may hold values from -0.1875 to 0.1875
- ffn_gain: float32 [2048], replicated, may hold values from 0.1 to 1.9
- w_shared_gate: bfloat16 [2048, 512], P(None, 'tp'), may hold values from -0.125 to 0.125
- w_shared_up: bfloat16 [2048, 512], P(None, 'tp'), may hold values from -0.125 to 0.125
- w_shared_down: bfloat16 [512, 2048], P('tp'), may hold values from -0.25 to 0.25
- routing: int32 [1024, 4], replicated, may hold values from 0 to 127, all different within a row; in each aligned block of 32 rows (0 to 31, 32 to 63, ...) at most 2 rows name the same one
- route_weights: float32 [1024, 4], P('ep'), may hold values from 0.1 to 1
- w_exp_gate: bfloat16 [128, 2048, 512], P(('ep', 'tp')), may hold values from -0.125 to 0.125
- w_exp_up: bfloat16 [128, 2048, 512], P(('ep', 'tp')), may hold values from -0.125 to 0.125
- w_exp_down: bfloat16 [128, 512, 2048], P(('ep', 'tp')), may hold values from -0.25 to 0.25
Outputs:
- mixed: bfloat16 [1024, 2048], P('ep', 'tp')
Inputs may be any that keep to these rules, and one draw needn't show every extreme that they name: `lengths`: A sequence's cache holds its past keys and values at positions below its length, and the new token follows them; some sequence uses all 1024 positions. `routing`: each row names 4 different experts. Within the rows of one group of 32 sequences (aligned blocks) no expert is named by more than 2 rows, and in some blocks an expert is named by exactly 2.
All inputs are finite; a program needn't handle non-finite values. No bound on the sum of `lengths` on one device may be relied on, other than what follows from the above.
Results may differ from a plain program's by a relative error of at most 0.015.
The roundings to bfloat16 on the way count: a program that leaves them out, or rounds other values in their place, can miss the bound.
Values may be sent and summed in bfloat16 or wider, within the bound.
A program may use at most 128 MiB of HBM per device.

v0:
```python
import jax
import jax.numpy as jnp
from jax import lax
from jax.sharding import PartitionSpec as P

epsilon = 1e-06
neg_fill = -1e30


def in_order(tiles, dim):
    tiles = jnp.moveaxis(tiles, 0, dim)
    lengths = tiles.shape
    return tiles.reshape(*lengths[:dim], lengths[dim] * lengths[dim + 1], *lengths[dim + 2 :])


def sent_to_all(shard, axis):
    copies = jnp.broadcast_to(shard, (lax.axis_size(axis), *shard.shape))
    return lax.all_to_all(copies, axis, split_axis=0, concat_axis=0, tiled=True)


def gathered_copies(shard, axis, dim):
    return in_order(sent_to_all(shard, axis), dim)


def cut_along(shard, dim, count):
    lengths = shard.shape
    tiles = shard.reshape(*lengths[:dim], count, lengths[dim] // count, *lengths[dim + 1 :])
    return jnp.moveaxis(tiles, dim, 0)


def sent_and_summed(shard, axis, dim):
    count = lax.axis_size(axis)
    tiles = lax.all_to_all(cut_along(shard, dim, count), axis, 0, 0, tiled=True)
    return jnp.sum(tiles.astype(jnp.float32), axis=0)


def norm_rows(values, gain_vec):
    widened = values.astype(jnp.float32)
    return (
        widened
        * lax.rsqrt(jnp.mean(widened * widened, axis=-1, keepdims=True) + epsilon)
        * gain_vec
    )


def attention(normed, kv_cache, lengths, w_query, w_key, w_value, lambdas, head_gain):
    seq_count = normed.shape[0]
    v_width = head_gain.shape[0]
    qk_width = v_width // 2
    kv_local = kv_cache.shape[2] // (2 * v_width)
    head_local = lambdas.shape[0]
    group_size = head_local // kv_local
    cache_len = kv_cache.shape[1]
    queries = jnp.dot(normed, w_query, preferred_element_type=jnp.float32).astype(jnp.bfloat16)
    queries = queries.reshape(seq_count, kv_local, group_size, 2, qk_width)
    key_new = jnp.dot(normed, w_key, preferred_element_type=jnp.float32).astype(jnp.bfloat16)
    key_new = key_new.reshape(seq_count, kv_local, 2, qk_width)
    value_new = jnp.dot(normed, w_value, preferred_element_type=jnp.float32).astype(jnp.bfloat16)
    value_new = value_new.reshape(seq_count, kv_local, v_width)
    layout = kv_cache.reshape(seq_count, cache_len, kv_local, 2 * v_width)
    keys_old = layout[..., :v_width].reshape(seq_count, cache_len, kv_local, 2, qk_width)
    values_old = layout[..., v_width:]
    scaling = qk_width ** (-0.5)
    scores_old = (
        jnp.einsum("skgmd,sckmd->skgmc", queries, keys_old, preferred_element_type=jnp.float32)
        * scaling
    )
    scores_new = (
        jnp.einsum("skgmd,skmd->skgm", queries, key_new, preferred_element_type=jnp.float32)
        * scaling
    )
    position = jnp.arange(cache_len, dtype=jnp.int32)
    valid_mask = (position[None, :] < lengths[:, None])[:, None, None, None, :]
    scores_old = jnp.where(valid_mask, scores_old, neg_fill)
    highest = jnp.maximum(jnp.max(scores_old, axis=-1), scores_new)
    expo_old = jnp.where(valid_mask, jnp.exp(scores_old - highest[..., None]), 0.0)
    expo_new = jnp.exp(scores_new - highest)
    totals = jnp.sum(expo_old, axis=-1) + expo_new
    lambda_grid = lambdas.reshape(kv_local, group_size)[None, :, :]
    weight_old = (
        expo_old[..., 0, :] / totals[..., 0, None]
        - lambda_grid[..., None] * expo_old[..., 1, :] / totals[..., 1, None]
    ).astype(jnp.bfloat16)
    weight_new = (
        expo_new[..., 0] / totals[..., 0] - lambda_grid * expo_new[..., 1] / totals[..., 1]
    ).astype(jnp.bfloat16)
    head_mix = jnp.einsum(
        "skgc,sckv->skgv", weight_old, values_old, preferred_element_type=jnp.float32
    )
    head_mix = (
        head_mix
        + weight_new.astype(jnp.float32)[..., None] * value_new.astype(jnp.float32)[:, :, None, :]
    )
    return (
        norm_rows(head_mix, head_gain).astype(jnp.bfloat16).reshape(seq_count, head_local * v_width)
    )


def shards(
    tokens,
    kv_cache,
    lengths,
    attn_gain,
    w_query,
    w_key,
    w_value,
    lambdas,
    head_gain,
    w_out,
    ffn_gain,
    w_shared_gate,
    w_shared_up,
    w_shared_down,
    routing,
    route_weights,
    w_exp_gate,
    w_exp_up,
    w_exp_down,
):
    seq_count = tokens.shape[0]
    width = tokens.shape[1]
    tp_count = lax.axis_size("tp")
    tp_index = lax.axis_index("tp")
    ep_count = lax.axis_size("ep")
    ep_index = lax.axis_index("ep")
    normed = norm_rows(tokens, attn_gain).astype(jnp.bfloat16)
    head_out = attention(normed, kv_cache, lengths, w_query, w_key, w_value, lambdas, head_gain)
    share_rows = head_out.shape[1]
    all_heads = gathered_copies(head_out, "tp", 1)
    pieces = jnp.einsum(
        "stk,tkd->tsd",
        all_heads.reshape(seq_count, tp_count, share_rows),
        w_out.reshape(tp_count, share_rows, -1),
        preferred_element_type=jnp.float32,
    )
    rounded = lax.optimization_barrier(pieces.astype(jnp.bfloat16))
    projected = jnp.sum(rounded.astype(jnp.float32), axis=0)
    residual = (tokens.astype(jnp.float32) + projected).astype(jnp.bfloat16)
    ffn_in = norm_rows(residual, ffn_gain).astype(jnp.bfloat16)
    gate_vals = jnp.dot(ffn_in, w_shared_gate, preferred_element_type=jnp.float32)
    up_vals = jnp.dot(ffn_in, w_shared_up, preferred_element_type=jnp.float32)
    shared_act = (jax.nn.silu(gate_vals) * up_vals).astype(jnp.bfloat16)
    shared_part = jnp.dot(shared_act, w_shared_down, preferred_element_type=jnp.float32)
    top_count = routing.shape[1]
    experts = w_exp_gate.shape[0] * ep_count * tp_count
    capacity = max(2, 2 * seq_count * top_count // experts)
    own_routing = lax.dynamic_slice_in_dim(routing, ep_index * seq_count, seq_count, 0)
    flat_ids = own_routing.reshape(-1)
    onehot = (flat_ids[:, None] == jnp.arange(experts, dtype=jnp.int32)[None, :]).astype(jnp.int32)
    slot_rank = jnp.sum((jnp.cumsum(onehot, axis=0) - onehot) * onehot, axis=1)
    in_column = flat_ids % tp_count == tp_index
    slot_ids = jnp.where(in_column, flat_ids // tp_count * capacity + slot_rank, -1)
    selector = (
        slot_ids[:, None] == jnp.arange(ep_count * capacity, dtype=jnp.int32)[None, :]
    ).astype(jnp.bfloat16)
    dispatch = jnp.sum(selector.reshape(seq_count, top_count, -1), axis=1)
    packed = jnp.einsum("sj,sd->jd", dispatch, ffn_in, preferred_element_type=jnp.float32).astype(
        jnp.bfloat16
    )
    packed = packed.reshape(ep_count, capacity, width)
    arrived = lax.all_to_all(packed, "ep", split_axis=0, concat_axis=0, tiled=True)
    flat_rows = arrived.reshape(-1, width)
    gate_part = jnp.dot(flat_rows, w_exp_gate[0], preferred_element_type=jnp.float32)
    up_part = jnp.dot(flat_rows, w_exp_up[0], preferred_element_type=jnp.float32)
    inner_act = (jax.nn.silu(gate_part) * up_part).astype(jnp.bfloat16)
    result = jnp.dot(inner_act, w_exp_down[0], preferred_element_type=jnp.float32).astype(
        jnp.bfloat16
    )
    computed = result.reshape(arrived.shape)
    returned = lax.all_to_all(computed, "ep", split_axis=0, concat_axis=0, tiled=True)
    routed_rows = jnp.dot(
        selector, returned.reshape(ep_count * capacity, width), preferred_element_type=jnp.float32
    ).reshape(seq_count, top_count, width)
    routed_part = jnp.sum(route_weights[:, :, None] * routed_rows, axis=1)
    combined = sent_and_summed((shared_part + routed_part).astype(jnp.bfloat16), "tp", 1)
    width_share = width // tp_count
    own_resid = lax.dynamic_slice_in_dim(residual, tp_index * width_share, width_share, 1).astype(
        jnp.float32
    )
    return (own_resid + combined).astype(jnp.bfloat16)


def solution(mesh):
    return jax.shard_map(
        shards,
        mesh=mesh,
        in_specs=(
            P("ep", None),
            P("ep", None, "tp"),
            P("ep"),
            P(),
            P(None, "tp"),
            P(None, "tp"),
            P(None, "tp"),
            P("tp"),
            P(),
            P(),
            P(),
            P(None, "tp"),
            P(None, "tp"),
            P("tp", None),
            P(),
            P("ep", None),
            P(("ep", "tp"), None, None),
            P(("ep", "tp"), None, None),
            P(("ep", "tp"), None, None),
        ),
        out_specs=P("ep", "tp"),
        check_vma=False,
    )
```

profile of v0, /device:TPU:1, one launch (start us, length us, event | category | flops | bytes accessed | tf_op | source)
XLA Modules:
  0.0 90.5 jit_solution(2187224256156566289)
XLA Ops:
  0.0 1.2 %fusion.28 = f32[32]{0:T(128)S(1)} fusion(bf16[32,2048]{1,0:T(8,128)(2,1)} %param.19), kind=kLoop, calls=%fused_computation.42 | loop fusion | flops 196576 | bytes 131200 | tf_op jit(solution)/shard_map/reduce_sum | solution.py:41
  1.2 1.6 %convolution_convert_fusion.3 = bf16[32,256]{1,0:T(8,128)(2,1)S(1)} fusion(bf16[2048,256]{1,0:T(8,128)(2,1)} %param.23, bf16[32,2048]{1,0:T(8,128)(2,1)} %param.19, f32[2048]{0:T(1024)} %param.22, f32[32]{0:T(128)S(1)} %add_rsqrt_fusion.2), kind=kOutput, calls=%fused_computation.21 | convolution fusion | flops 33824768 | bytes 1204352 | tf_op jit(solution)/shard_map/dot_general | solution.py:54
  3.0 11.9 %copy.63 = bf16[32,1024,128]{1,2,0:T(8,128)(2,1)} copy(bf16[32,1024,128]{2,1,0:T(8,128)(2,1)} %param.20) | data formatting | bytes 16777216 | tf_op args[1]
  14.9 2.6 %slice.34 = bf16[32,1024,1,64]{1,3,0,2:T(8,128)(2,1)S(1)} slice(bf16[32,1024,1,128]{1,3,0,2:T(8,128)(2,1)} %bitcast.124), slice={[0:32], [0:1024], [0:1], [0:64]} | slice | bytes 8388608 | tf_op jit(solution)/shard_map/slice | solution.py:61
  17.7 1.0 %fusion.81 = (f32[32,4,2]{1,2,0:T(2,128)S(1)}, f32[32,1,4,2,1024]{4,2,3,0,1:T(4,128)S(1)}) fusion(bf16[32,1024,2,32]{1,3,2,0:T(8,128)(2,1)S(1)} %bitcast.126, bf16[32,4,2,32]{3,2,1,0:T(2,128)(2,1)S(1)} %reshape.251, pred[32,1024]{1,0:T(8,128)(4,1)S(1)} %iota_compare_fusion), kind=kOutput, calls=%fused_computation.114 | convolution fusion | flops 17563392 | bytes 5293056 | tf_op jit(solution)/shard_map/skgmd,sckmd->skgmc/dot_general | solution.py:65
  18.8 1.2 %convolution_convert_fusion.5 = bf16[32,64]{1,0:T(8,128)(2,1)S(1)} fusion(bf16[2048,64]{0,1:T(8,128)(2,1)} %param.24, bf16[32,2048]{1,0:T(8,128)(2,1)S(1)} %copy-done.1, f32[2048]{0:T(1024)S(1)} %copy-done.4, f32[32]{0:T(128)S(1)} %add_rsqrt_fusion.2), kind=kOutput, calls=%fused_computation.26 | convolution fusion | flops 8652800 | bytes 405632 | tf_op jit(solution)/shard_map/dot_general | solution.py:56
  20.5 1.7 %fusion.80 = (f32[32,4,2]{1,2,0:T(2,128)S(1)}, f32[32,1,4,2,1024]{4,2,3,0,1:T(4,128)}) fusion(f32[32,1,4,2,1024]{4,2,3,0,1:T(4,128)S(1)} %get-tuple-element.15, f32[32,4,2]{1,2,0:T(2,128)S(1)} %copy.66, pred[32,1024]{1,0:T(8,128)(4,1)S(1)} %iota_compare_fusion), kind=kLoop, calls=%fused_computation.113 | loop fusion | flops 786176 | bytes 2131968 | tf_op jit(solution)/shard_map/reduce_sum | solution.py:78
  22.6 1.2 %fusion.21 = f32[32,64]{1,0:T(8,128)S(1)} fusion(bf16[2048,64]{0,1:T(8,128)(2,1)} %param.25, bf16[32,2048]{1,0:T(8,128)(2,1)S(1)} %copy-done.1, f32[2048]{0:T(1024)S(1)} %copy-done.4, f32[32]{0:T(128)S(1)} %add_rsqrt_fusion.2), kind=kOutput, calls=%fused_computation.25 | convolution fusion | flops 8654848 | bytes 409728 | tf_op jit(solution)/shard_map/dot_general | solution.py:58
  23.9 3.9 %multiply_reduce_fusion = (f32[32,4]{1,0:T(8,128)S(1)}, f32[32,4,64]{2,1,0:T(4,128)S(1)}) fusion(f32[32,64]{1,0:T(8,128)S(1)} %fusion.21, f32[32,4]{1,0:T(8,128)S(1)} %copy.71, bf16[32,1024,1,128]{1,3,0,2:T(8,128)(2,1)} %bitcast.125, f32[32,1,4,2,1024]{4,2,3,0,1:T(4,128)} %get-tuple-element.10, f32[32,4]{1,0:T(8,128)S(1)} %copy.70, f32[4]{0:T(128)S(1)} %copy-done.7, ...), kind=kOutput, calls=%fused_computation.66 | convolution fusion | flops 17465216 | bytes 5285904 | tf_op jit(solution)/shard_map/skgc,sckv->skgv/dot_general | solution.py:87
  28.6 4.8 %all-to-all-start = ((bf16[4,32,256]{2,1,0:T(8,128)(2,1)}), bf16[4,32,256]{2,1,0:T(8,128)(2,1)S(1)}, u32[]{:S(2)}, u32[]{:S(2)}) async-start(bf16[4,32,256]{2,1,0:T(8,128)(2,1)} %broadcast_in_dim.45), calls=%async_computation | async-start | bytes 131072 | tf_op jit(solution)/shard_map/all_to_all | solution.py:18
  33.5 0.8 constant_dynamic-slice_fusion
  35.2 2.8 %all-to-all-done = bf16[4,32,256]{2,1,0:T(8,128)(2,1)S(1)} async-done(((bf16[4,32,256]{2,1,0:T(8,128)(2,1)}), bf16[4,32,256]{2,1,0:T(8,128)(2,1)S(1)}, u32[]{:S(2)}, u32[]{:S(2)}) %all-to-all-start) | async-done | bytes 65568 | tf_op jit(solution)/shard_map/all_to_all | solution.py:18
  37.9 3.0 %convolution_convert_fusion = bf16[4,32,2048]{2,1,0:T(8,128)(2,1)S(1)} fusion(bf16[4,256,2048]{2,1,0:T(8,128)(2,1)} %bitcast.127, bf16[4,32,256]{2,1,0:T(8,128)(2,1)S(1)} %all-to-all-done), kind=kOutput, calls=%fused_computation.3 | convolution fusion | flops 134479872 | bytes 4784128 | tf_op jit(solution)/shard_map/stk,tkd->tsd/dot_general | solution.py:130
  41.7 18.9 %all_to_all.20 = bf16[32,2,2048]{2,1,0:T(2,128)(2,1)S(1)} all-to-all(bf16[32,2,2048]{2,1,0:T(2,128)(2,1)S(1)} %reshape.258), channel_id=1, replica_groups=mesh['ep'=32,'tp'=4] {'ep'}, dimensions={0} | all-to-all | bytes 524288 | tf_op jit(solution)/shard_map/all_to_all | solution.py:161
  60.7 2.1 %fusion.5 = f32[64,512]{1,0:T(8,128)S(1)} fusion(bf16[64,2048]{1,0:T(8,128)(2,1)S(1)} %reshape.259, bf16[1,2048,512]{2,1,0:T(8,128)(2,1)} %param.35), kind=kOutput, calls=%fused_computation.11 | convolution fusion | flops 134217728 | bytes 2490368 | tf_op jit(solution)/shard_map/dot_general | solution.py:163
  62.8 2.5 %convolution_convert_fusion.1 = bf16[64,2048]{1,0:T(8,128)(2,1)S(1)} fusion(bf16[1,512,2048]{2,1,0:T(8,128)(2,1)S(1)} %copy-done, bf16[64,2048]{1,0:T(8,128)(2,1)S(1)} %reshape.259, bf16[1,2048,512]{2,1,0:T(8,128)(2,1)} %param.36, f32[64,512]{1,0:T(8,128)S(1)} %fusion.5), kind=kOutput, calls=%fused_computation.4 | convolution fusion | flops 268763136 | bytes 4849664 | tf_op jit(solution)/shard_map/dot_general | solution.py:166
  65.3 0.9 reshape.260
  66.2 3.8 %all-to-all-start.2 = ((bf16[32,2,2048]{2,1,0:T(2,128)(2,1)}), bf16[32,2,2048]{2,1,0:T(2,128)(2,1)S(1)}, u32[]{:S(2)}, u32[]{:S(2)}) async-start(bf16[32,2,2048]{2,1,0:T(2,128)(2,1)} %reshape.260), calls=%async_computation.2 | async-start | bytes 524288 | tf_op jit(solution)/shard_map/all_to_all | solution.py:170
  70.3 8.6 %all-to-all-done.2 = bf16[32,2,2048]{2,1,0:T(2,128)(2,1)S(1)} async-done(((bf16[32,2,2048]{2,1,0:T(2,128)(2,1)}), bf16[32,2,2048]{2,1,0:T(2,128)(2,1)S(1)}, u32[]{:S(2)}, u32[]{:S(2)}) %all-to-all-start.2) | async-done | bytes 262176 | tf_op jit(solution)/shard_map/all_to_all | solution.py:170
  79.3 1.6 %fusion.1 = bf16[32,2048]{1,0:T(8,128)(2,1)S(1)} fusion(f32[32,2048]{1,0:T(8,128)S(1)} %fusion.8, bf16[128,2048]{1,0:T(8,128)(2,1)} %param.32, bf16[2048,128]{1,0:T(8,128)(2,1)} %param.31, f32[32,128]{1,0:T(8,128)S(1)} %fusion.76, bf16[32,2048]{1,0:T(8,128)(2,1)S(1)} %get-tuple-element.6, f32[2048]{0:T(1024)S(1)} %copy-done.3, f32[32]{0:T(128)S(1)} %add_rsqrt_fusion.1), kind=kOutput, calls=%fused_computation.7 | convolution fusion | flops 33972224 | bytes 1597568 | tf_op jit(solution)/shard_map/dot_general | solution.py:143
  81.0 0.7 copy.88
  81.7 3.3 %all-to-all-start.3 = ((bf16[4,32,512]{2,1,0:T(8,128)(2,1)}), bf16[4,32,512]{2,1,0:T(8,128)(2,1)S(1)}, u32[]{:S(2)}, u32[]{:S(2)}) async-start(bf16[4,32,512]{2,1,0:T(8,128)(2,1)} %bitcast.123), calls=%async_computation.3 | async-start | bytes 262144 | tf_op jit(solution)/shard_map/all_to_all | solution.py:33
  85.0 4.9 %all-to-all-done.3 = bf16[4,32,512]{2,1,0:T(8,128)(2,1)S(1)} async-done(((bf16[4,32,512]{2,1,0:T(8,128)(2,1)}), bf16[4,32,512]{2,1,0:T(8,128)(2,1)S(1)}, u32[]{:S(2)}, u32[]{:S(2)}) %all-to-all-start.3) | async-done | bytes 131104 | tf_op jit(solution)/shard_map/all_to_all | solution.py:33
  89.9 0.6 add_convert_fusion
  (56 shorter events, 4.6 us)
Async XLA Ops:
  0.0 62.8 %copy-start = (bf16[1,512,2048]{2,1,0:T(8,128)(2,1)S(1)}, bf16[1,512,2048]{2,1,0:T(8,128)(2,1)}, u32[]{:S(2)}) copy-start(bf16[1,512,2048]{2,1,0:T(8,128)(2,1)} %param.37) | copy-start | bytes 6291460
  14.9 2.7 %copy-start.5 = (s32[32]{0:T(128)S(1)}, s32[32]{0:T(128)}, u32[]{:S(2)}) copy-start(s32[32]{0:T(128)} %param.21) | copy-start | bytes 388
  17.6 1.2 %copy-start.1 = (bf16[32,2048]{1,0:T(8,128)(2,1)S(1)}, bf16[32,2048]{1,0:T(8,128)(2,1)}, u32[]{:S(2)}) copy-start(bf16[32,2048]{1,0:T(8,128)(2,1)} %param.19) | copy-start | bytes 393220
  17.6 1.2 %copy-start.4 = (f32[2048]{0:T(1024)S(1)}, f32[2048]{0:T(1024)}, u32[]{:S(2)}) copy-start(f32[2048]{0:T(1024)} %param.22) | copy-start | bytes 24580
  17.7 4.6 %copy-start.7 = (f32[4]{0:T(128)S(1)}, f32[4]{0:T(128)}, u32[]{:S(2)}) copy-start(f32[4]{0:T(128)} %param.26) | copy-start | bytes 52
  23.9 3.9 %copy-start.6 = (f32[64]{0:T(128)S(1)}, f32[64]{0:T(128)}, u32[]{:S(2)}) copy-start(f32[64]{0:T(128)} %param.27) | copy-start | bytes 772
  28.6 9.3 %all-to-all-start = ((bf16[4,32,256]{2,1,0:T(8,128)(2,1)}), bf16[4,32,256]{2,1,0:T(8,128)(2,1)S(1)}, u32[]{:S(2)}, u32[]{:S(2)}) async-start(bf16[4,32,256]{2,1,0:T(8,128)(2,1)} %broadcast_in_dim.45), calls=%async_computation | async-start | bytes 131072 | tf_op jit(solution)/shard_map/all_to_all | solution.py:18
  37.9 3.3 %copy-start.3 = (f32[2048]{0:T(1024)S(1)}, f32[2048]{0:T(1024)}, u32[]{:S(2)}) copy-start(f32[2048]{0:T(1024)} %param.29) | copy-start | bytes 24580
  60.7 9.3 %copy-start.2 = (bf16[2048,128]{1,0:T(8,128)(2,1)S(1)}, bf16[2048,128]{1,0:T(8,128)(2,1)}, u32[]{:S(2)}) copy-start(bf16[2048,128]{1,0:T(8,128)(2,1)} %param.30) | copy-start | bytes 1572868
  60.7 18.3 %copy-start.8 = (f32[32,4]{0,1:T(4,128)S(1)}, f32[32,4]{0,1:T(4,128)}, u32[]{:S(2)}) copy-start(f32[32,4]{0,1:T(4,128)} %param.34) | copy-start | bytes 1540
  66.2 12.7 %all-to-all-start.2 = ((bf16[32,2,2048]{2,1,0:T(2,128)(2,1)}), bf16[32,2,2048]{2,1,0:T(2,128)(2,1)S(1)}, u32[]{:S(2)}, u32[]{:S(2)}) async-start(bf16[32,2,2048]{2,1,0:T(2,128)(2,1)} %reshape.260), calls=%async_computation.2 | async-start | bytes 524288 | tf_op jit(solution)/shard_map/all_to_all | solution.py:170
  81.7 8.2 %all-to-all-start.3 = ((bf16[4,32,512]{2,1,0:T(8,128)(2,1)}), bf16[4,32,512]{2,1,0:T(8,128)(2,1)S(1)}, u32[]{:S(2)}, u32[]{:S(2)}) async-start(bf16[4,32,512]{2,1,0:T(8,128)(2,1)} %bitcast.123), calls=%async_computation.3 | async-start | bytes 262144 | tf_op jit(solution)/shard_map/all_to_all | solution.py:33
where the time goes:
time: 91.5 us; the launch traced here: 90.5 us
  local copies, waits for them, and re-layouts  19.3 us (21%)
  matrix products  19.3 us (21%)
  blocking collectives  18.9 us (21%)
  waiting for transfers between devices  16.3 us (18%)
  starting transfers between devices  11.9 us (13%)
  other arithmetic  4.63 us (5%)
    all_to_all x1, blocking collectives, shards(): lax.all_to_all(packed, 'ep', split_axis=0, concat_axis=0, tiled=True)  18.9 us
    unnamed x20, local copies, waits for them, and re-layouts  12.1 us
    all_to_all x1, waiting for transfers between devices, shards(): lax.all_to_all(computed, 'ep', split_axis=0, concat_axis=0, tiled=True)  8.62 us
    all_to_all x1, waiting for transfers between devices, sent_and_summed(): tiles = lax.all_to_all(cut_along(shard, dim, count), axis, 0, 0, tiled=True)  4.89 us
    all_to_all x1, starting transfers between devices, sent_to_all(): return lax.all_to_all(copies, axis, split_axis=0, concat_axis=0, tiled=True)  4.83 us
    dot_general x1, matrix products, attention(): jnp.einsum('skgc,sckv->skgv', weight_old, values_old, preferred_element_t...  3.87 us
    all_to_all x1, starting transfers between devices, shards(): lax.all_to_all(computed, 'ep', split_axis=0, concat_axis=0, tiled=True)  3.75 us
    all_to_all x1, starting transfers between devices, sent_and_summed(): tiles = lax.all_to_all(cut_along(shard, dim, count), axis, 0, 0, tiled=True)  3.32 us
  transfers between devices with their start and end apart: 3, of which 3 were waited for; matrix products, arithmetic and copies ran while one was open for 2% of the time, Pallas kernels for 0%

commit v1 on v0

v1 whole, which is shorter than its diff:
```python
import jax
import jax.numpy as jnp
from jax import lax
from jax.experimental import pallas as pl
from jax.experimental.pallas import tpu as pltpu
from jax.sharding import PartitionSpec as P

MESH = pl.DeviceIdType.MESH
EPS = 1e-06
NEG = -1e30
F32 = jnp.float32
BF16 = jnp.bfloat16
CHUNKS = 4


def iota(shape, dim):
    return lax.broadcasted_iota(jnp.int32, shape, dim)


def dot(a, b):
    return jnp.dot(a, b, preferred_element_type=F32)


def dot_ta(a, b):
    return lax.dot_general(a, b, (((0,), (0,)), ((), ())), preferred_element_type=F32)


def layer(
    n_ep,
    n_tp,
    tokens_h,
    kv_h,
    lengths_s,
    attn_gain_h,
    wq_h,
    wk_h,
    wv_h,
    lambdas_s,
    head_gain_h,
    wo_h,
    ffn_gain_h,
    wsg_h,
    wsu_h,
    wsd_h,
    routing_h,
    rw_h,
    wg_h,
    wu_h,
    wd_h,
    out_ref,
    tokens_v,
    kv_v,
    attn_gain_v,
    wq_v,
    wk_v,
    wv_v,
    head_gain_v,
    wo_v,
    ffn_gain_v,
    wsg_v,
    wsu_v,
    wsd_v,
    routing_v,
    rw_v,
    wg_v,
    wu_v,
    wd_v,
    qblk_v,
    kvn_v,
    sc_v,
    wt_v,
    acc_v,
    ho_v,
    proj_v,
    resid_v,
    oh_v,
    fold_v,
    m2_v,
    send1_v,
    recv1_v,
    shs_v,
    shr_v,
    send2_v,
    recv2_v,
    lsem,
    ksem,
    ho_ss,
    ho_rs,
    d_ss,
    d_rs,
    sh_ss,
    sh_rs,
    r_ss,
    r_rs,
):
    ep = lax.axis_index("ep")
    tp = lax.axis_index("tp")
    n_dev = n_ep * n_tp
    me = ep * n_tp + tp
    seqs, width = tokens_v.shape
    cache = kv_v.shape[1]
    chunk = cache // CHUNKS
    heads = 4
    qk = 32
    rows = heads * seqs

    order = [
        (tokens_h, tokens_v),
        (attn_gain_h, attn_gain_v),
        (wq_h, wq_v),
        (wk_h, wk_v),
        (wv_h, wv_v),
        (routing_h.at[pl.ds(pl.multiple_of(ep * seqs, 8), seqs)], routing_v),
        (rw_h, rw_v),
        (head_gain_h, head_gain_v),
        (ffn_gain_h, ffn_gain_v),
        (wo_h, wo_v),
        (wsg_h, wsg_v),
        (wsu_h, wsu_v),
        (wsd_h, wsd_v),
        (wg_h.at[0], wg_v),
        (wu_h.at[0], wu_v),
        (wd_h.at[0], wd_v),
    ]
    copies = [pltpu.make_async_copy(a, b, lsem.at[i]) for i, (a, b) in enumerate(order)]
    for copy in copies[:9]:
        copy.start()
    kv_copies = []
    for c in range(CHUNKS):
        part = pl.ds(c * chunk, chunk)
        kv_copies.append(
            pltpu.make_async_copy(kv_h.at[:, part, :], kv_v.at[:, part, :], ksem.at[c])
        )
    for copy in kv_copies:
        copy.start()
    for copy in copies[9:]:
        copy.start()

    barrier = pltpu.get_barrier_semaphore()

    def greet(d, carry):
        other = lax.rem(me + d, n_dev)
        pl.semaphore_signal(
            barrier,
            inc=1,
            device_id=(lax.div(other, n_tp), lax.rem(other, n_tp)),
            device_id_type=MESH,
        )
        return carry

    lax.fori_loop(1, n_dev, greet, 0)

    qblk_v[...] = jnp.zeros_like(qblk_v)

    copies[0].wait()
    copies[1].wait()
    tok = tokens_v[...].astype(F32)
    mean = jnp.mean(tok * tok, axis=-1, keepdims=True)
    normed = (tok * lax.rsqrt(mean + EPS) * attn_gain_v[...]).astype(BF16)
    copies[2].wait()
    q = dot(normed, wq_v[...]).astype(BF16)
    copies[3].wait()
    kn = dot(normed, wk_v[...])
    copies[4].wait()
    vn = dot(normed, wv_v[...])
    new_kv = jnp.concatenate([kn, vn], axis=1)

    spread = (
        iota((seqs, heads * rows), 1)
        == iota((seqs, heads * rows), 0)
        + (iota((seqs, heads * rows), 1) // rows) * (rows + seqs)
    ).astype(BF16)
    wide = dot_ta(q, spread)
    qt = wide[0 : 2 * qk, 0:rows]
    for h in range(1, heads):
        qt = qt + wide[h * 2 * qk : (h + 1) * 2 * qk, h * rows : (h + 1) * rows]
    lane_seq = lax.rem(iota((2 * qk, rows), 1), seqs)
    for s in range(seqs):
        block = jnp.where(lane_seq == s, qt, 0.0).astype(BF16)
        qblk_v[s * 128 : s * 128 + qk, 0:rows] = block[0:qk]
        qblk_v[s * 128 + qk : s * 128 + 2 * qk, rows : 2 * rows] = block[qk : 2 * qk]
        kvn_v[s] = jnp.broadcast_to(new_kv[s : s + 1, :], (16, 128)).astype(BF16)

    lane1 = iota((1, 2 * rows), 1)
    len_lane = jnp.zeros((1, 2 * rows), jnp.int32)
    for s in range(seqs):
        len_lane = jnp.where(lax.rem(lane1, seqs) == s, lengths_s[s], len_lane)
    lane_head = iota((1, rows), 1) // seqs
    lam_lane = jnp.zeros((1, rows), F32)
    for h in range(heads):
        lam_lane = jnp.where(lane_head == h, lambdas_s[h], lam_lane)

    lhs_new = jnp.concatenate([kvn_v[s] for s in range(seqs)], axis=1)
    sc_new = dot(lhs_new, qblk_v[...])
    sc_new = jnp.where(iota((16, 2 * rows), 0) == 0, sc_new, NEG)
    top = jnp.max(sc_new, axis=0, keepdims=True)
    for c in range(CHUNKS):
        kv_copies[c].wait()
        part = pl.ds(c * chunk, chunk)
        lhs = jnp.concatenate([kv_v[s, part, :] for s in range(seqs)], axis=1)
        sc = dot(lhs, qblk_v[...])
        valid = iota((chunk, 2 * rows), 0) + c * chunk < len_lane
        sc = jnp.where(valid, sc, NEG)
        sc_v[part, :] = sc
        top = jnp.maximum(top, jnp.max(sc, axis=0, keepdims=True))

    scaling = qk ** (-0.5)
    ex_new = jnp.exp((sc_new - top) * scaling)
    total = jnp.sum(ex_new, axis=0, keepdims=True)
    for c in range(CHUNKS):
        part = pl.ds(c * chunk, chunk)
        ex = jnp.exp((sc_v[part, :] - top) * scaling)
        sc_v[part, :] = ex
        total = total + jnp.sum(ex, axis=0, keepdims=True)
    inv = 1.0 / total
    inv1 = inv[:, 0:rows]
    inv2 = inv[:, rows : 2 * rows] * lam_lane
    w_new = ex_new[:, 0:rows] * inv1 - ex_new[:, rows : 2 * rows] * inv2
    wt_new = jnp.concatenate([w_new, jnp.zeros((112, rows), F32)], axis=0).T.astype(BF16)
    for c in range(CHUNKS):
        part = pl.ds(c * chunk, chunk)
        w = sc_v[part, 0:rows] * inv1 - sc_v[part, rows : 2 * rows] * inv2
        wt_v[:, part] = w.T.astype(BF16)

    acc_v[...] = jnp.zeros_like(acc_v)
    row_seq = lax.rem(iota((rows, 128), 0), seqs)

    def mix(p, carry):
        base = p * 4
        rhs = jnp.concatenate([kv_v[base + i] for i in range(4)], axis=1)
        rhs_new = jnp.concatenate([kvn_v[base + i] for i in range(4)], axis=1)
        o = dot(wt_v[...], rhs) + dot(wt_new[:, 0:16], rhs_new)
        acc = acc_v[...]
        for i in range(4):
            acc = jnp.where(row_seq == base + i, o[:, i * 128 : (i + 1) * 128], acc)
        acc_v[...] = acc
        return carry

    lax.fori_loop(0, seqs // 4, mix, 0)

    upper = iota((rows, 128), 1) >= 64
    mixv = jnp.where(upper, acc_v[...], 0.0)
    copies[7].wait()
    ms = jnp.sum(mixv * mixv, axis=-1, keepdims=True) * (1.0 / 64.0)
    ho = mixv * lax.rsqrt(ms + EPS) * head_gain_v[...]
    low = iota((seqs, 128), 1) < 64
    halves = []
    for i in range(2):
        even = ho[(2 * i) * seqs : (2 * i + 1) * seqs]
        odd = ho[(2 * i + 1) * seqs : (2 * i + 2) * seqs]
        halves.append(jnp.where(low, pltpu.roll(even, 64, 1), odd))
    head_out = jnp.concatenate(halves, axis=1).astype(BF16)
    ho_v[tp] = head_out

    pl.semaphore_wait(barrier, n_dev - 1)
    ho_copies = []
    for d in range(1, n_tp):
        copy = pltpu.make_async_remote_copy(
            src_ref=ho_v.at[tp],
            dst_ref=ho_v.at[tp],
            send_sem=ho_ss.at[d],
            recv_sem=ho_rs.at[d],
            device_id=(ep, lax.rem(tp + d, n_tp)),
            device_id_type=MESH,
        )
        copy.start()
        ho_copies.append(copy)

    copies[5].wait()
    copies[6].wait()
    e_lane = iota((seqs, n_dev), 1)
    picks = [routing_v[:, k : k + 1] for k in range(4)]
    hots = [(e_lane == r).astype(F32) for r in picks]
    named = hots[0] + hots[1] + hots[2] + hots[3]
    earlier = (iota((seqs, seqs), 1) < iota((seqs, seqs), 0)).astype(BF16)
    before = dot(earlier, named.astype(BF16))
    ranks = [jnp.sum(h * before, axis=1, keepdims=True).astype(jnp.int32) for h in hots]
    d_col = iota((seqs, n_ep * 8), 1)
    pieces = []
    for a in range(4):
        piece = jnp.zeros((seqs, n_ep * 8), F32)
        for k in range(4):
            slot = (picks[k] // n_tp) * 8 + ranks[k] * 4 + a
            slot = jnp.where(lax.rem(picks[k], n_tp) == tp, slot, -1)
            piece = piece + (d_col == slot).astype(F32)
        pieces.append(piece)
    oh_v[...] = jnp.concatenate(pieces, axis=0).T.astype(BF16)
    m_col = iota((seqs, n_dev * 8), 1)
    for b in range(4):
        piece = jnp.zeros((seqs, n_dev * 8), F32)
        for k in range(4):
            slot = picks[k] * 8 + ranks[k] * 4 + b
            piece = jnp.where(m_col == slot, rw_v[:, k : k + 1], piece)
        high = piece.astype(BF16)
        m2_v[b * seqs : (b + 1) * seqs, :] = high
        m2_v[(4 + b) * seqs : (5 + b) * seqs, :] = (piece - high.astype(F32)).astype(BF16)
    sq = n_ep * 8
    i0, i1 = iota((sq, sq), 0), iota((sq, sq), 1)
    fold_v[0] = (i1 == lax.rem(i0, sq // 4) * 4 + i0 // (sq // 4)).astype(BF16)
    fold_v[1] = (i1 == lax.rem(i0, 4) * (sq // 4) + i0 // 4).astype(BF16)

    copies[9].wait()
    share = heads * 64

    def project(owner):
        part = dot(ho_v[owner], wo_v[pl.ds(pl.multiple_of(owner * share, share), share), :])
        return part.astype(BF16).astype(F32)

    proj_v[...] = project(tp)
    for d in (1, 3, 2):
        ho_copies[d - 1].wait_recv()
        owner = lax.rem(tp + n_tp - d, n_tp)
        proj_v[...] += project(owner)
    copies[8].wait()
    resid = (tokens_v[...].astype(F32) + proj_v[...]).astype(BF16)
    quarter = width // n_tp
    for t in range(n_tp):
        resid_v[t] = resid[:, t * quarter : (t + 1) * quarter]
    rf = resid.astype(F32)
    mean = jnp.mean(rf * rf, axis=-1, keepdims=True)
    ffn_in = (rf * lax.rsqrt(mean + EPS) * ffn_gain_v[...]).astype(BF16)

    folded = jnp.concatenate(
        [ffn_in[:, a * quarter : (a + 1) * quarter] for a in range(4)], axis=0
    )
    packed = dot(oh_v[...], folded).astype(BF16)
    send1_v[...] = packed.reshape(send1_v.shape)
    recv1_v[ep] = send1_v[ep]

    def dispatch(d, carry):
        other = lax.rem(ep + d, n_ep)
        pltpu.make_async_remote_copy(
            src_ref=send1_v.at[other],
            dst_ref=recv1_v.at[ep],
            send_sem=d_ss,
            recv_sem=d_rs,
            device_id=(other, tp),
            device_id_type=MESH,
        ).start()
        return carry

    lax.fori_loop(1, n_ep, dispatch, 0)

    copies[10].wait()
    copies[11].wait()
    copies[12].wait()
    gate = dot(ffn_in, wsg_v[...])
    up = dot(ffn_in, wsu_v[...])
    act = (gate / (1.0 + jnp.exp(-gate)) * up).astype(BF16)
    part = dot(act, wsd_v[...]).astype(BF16)
    for t in range(n_tp):
        shs_v[t] = part[:, t * quarter : (t + 1) * quarter]
    sh_copies = []
    for d in range(1, n_tp):
        other = lax.rem(tp + d, n_tp)
        copy = pltpu.make_async_remote_copy(
            src_ref=shs_v.at[other],
            dst_ref=shr_v.at[d],
            send_sem=sh_ss.at[d],
            recv_sem=sh_rs.at[d],
            device_id=(ep, other),
            device_id_type=MESH,
        )
        copy.start()
        sh_copies.append(copy)

    copies[13].wait()
    copies[14].wait()
    copies[15].wait()
    arrived = recv1_v.at[pl.ds(0, n_ep - 1)]
    pltpu.make_async_copy(arrived, arrived, d_rs).wait()
    flat = dot(fold_v[0], recv1_v[...].reshape(sq, quarter)).astype(BF16)
    n_rows = sq // 4
    lhs = jnp.concatenate([flat[a * n_rows : (a + 1) * n_rows] for a in range(4)], axis=1)
    gate = dot(lhs, wg_v[...])
    up = dot(lhs, wu_v[...])
    act = (gate / (1.0 + jnp.exp(-gate)) * up).astype(BF16)
    res = dot(act, wd_v[...]).astype(BF16)
    stacked = jnp.concatenate(
        [
            jnp.concatenate(
                [
                    res[:, t * quarter + b * 128 : t * quarter + (b + 1) * 128]
                    for t in range(n_tp)
                ],
                axis=1,
            )
            for b in range(4)
        ],
        axis=0,
    )
    back = dot(fold_v[1], stacked).astype(BF16)
    for t in range(n_tp):
        send2_v[:, t] = back[:, t * 128 : (t + 1) * 128].reshape(n_ep, 8, 128)
    recv2_v[me] = send2_v[ep, tp]

    def give_back(d, carry):
        other = lax.rem(me + d, n_dev)
        oe, ot = lax.div(other, n_tp), lax.rem(other, n_tp)
        pltpu.make_async_remote_copy(
            src_ref=send2_v.at[oe, ot],
            dst_ref=recv2_v.at[me],
            send_sem=r_ss,
            recv_sem=r_rs,
            device_id=(oe, ot),
            device_id_type=MESH,
        ).start()
        return carry

    lax.fori_loop(1, n_dev, give_back, 0)

    final = resid_v[tp].astype(F32) + shs_v[tp].astype(F32)
    for copy in sh_copies:
        copy.wait_recv()
    for d in range(1, n_tp):
        final = final + shr_v[d].astype(F32)
    back_all = recv2_v.at[pl.ds(0, n_dev - 1)]
    pltpu.make_async_copy(back_all, back_all, r_rs).wait()
    routed = dot(m2_v[...], recv2_v[...].reshape(n_dev * 8, 128))
    half = 4 * seqs
    routed = routed[0:half] + routed[half : 2 * half]
    final = final + jnp.concatenate(
        [routed[b * seqs : (b + 1) * seqs] for b in range(4)], axis=1
    )
    out_ref[...] = final.astype(BF16)

    for copy in ho_copies:
        copy.wait_send()
    for copy in sh_copies:
        copy.wait_send()
    sent = send1_v.at[pl.ds(0, n_ep - 1)]
    pltpu.make_async_copy(sent, sent, d_ss).wait()
    pltpu.make_async_copy(back_all, back_all, r_ss).wait()


def solution(mesh):
    n_ep, n_tp = mesh.shape["ep"], mesh.shape["tp"]

    def shards(
        tokens,
        kv_cache,
        lengths,
        attn_gain,
        w_query,
        w_key,
        w_value,
        lambdas,
        head_gain,
        w_out,
        ffn_gain,
        w_shared_gate,
        w_shared_up,
        w_shared_down,
        routing,
        route_weights,
        w_exp_gate,
        w_exp_up,
        w_exp_down,
    ):
        seqs, width = tokens.shape
        n_dev = n_ep * n_tp
        quarter = width // n_tp
        rows = 4 * seqs
        gain2 = jnp.concatenate([head_gain, head_gain]).reshape(1, -1)
        args = (
            tokens,
            kv_cache,
            lengths,
            attn_gain.reshape(1, -1),
            w_query,
            w_key,
            w_value,
            lambdas,
            gain2,
            w_out,
            ffn_gain.reshape(1, -1),
            w_shared_gate,
            w_shared_up,
            w_shared_down,
            routing,
            route_weights,
            w_exp_gate,
            w_exp_up,
            w_exp_down,
        )
        anyspec = pl.BlockSpec(memory_space=pl.ANY)
        smem = pl.BlockSpec(memory_space=pltpu.SMEM)
        specs = [anyspec] * len(args)
        specs[2] = smem
        specs[7] = smem

        def vm(a):
            return pltpu.VMEM(a.shape, a.dtype)

        scratch = [
            vm(tokens),
            vm(kv_cache),
            pltpu.VMEM((1, width), F32),
            vm(w_query),
            vm(w_key),
            vm(w_value),
            pltpu.VMEM((1, 128), F32),
            vm(w_out),
            pltpu.VMEM((1, width), F32),
            vm(w_shared_gate),
            vm(w_shared_up),
            vm(w_shared_down),
            pltpu.VMEM((seqs, 4), jnp.int32),
            vm(route_weights),
            pltpu.VMEM(w_exp_gate.shape[1:], BF16),
            pltpu.VMEM(w_exp_up.shape[1:], BF16),
            pltpu.VMEM(w_exp_down.shape[1:], BF16),
            pltpu.VMEM((seqs * 128, 2 * rows), BF16),
            pltpu.VMEM((seqs, 16, 128), BF16),
            pltpu.VMEM((kv_cache.shape[1], 2 * rows), F32),
            pltpu.VMEM((rows, kv_cache.shape[1]), BF16),
            pltpu.VMEM((rows, 128), F32),
            pltpu.VMEM((n_tp, seqs, 256), BF16),
            pltpu.VMEM((seqs, width), F32),
            pltpu.VMEM((n_tp, seqs, quarter), BF16),
            pltpu.VMEM((n_ep * 8, 4 * seqs), BF16),
            pltpu.VMEM((2, n_ep * 8, n_ep * 8), BF16),
            pltpu.VMEM((8 * seqs, n_dev * 8), BF16),
            pltpu.VMEM((n_ep, 8, quarter), BF16),
            pltpu.VMEM((n_ep, 8, quarter), BF16),
            pltpu.VMEM((n_tp, seqs, quarter), BF16),
            pltpu.VMEM((n_tp, seqs, quarter), BF16),
            pltpu.VMEM((n_ep, n_tp, 8, 128), BF16),
            pltpu.VMEM((n_dev, 8, 128), BF16),
            pltpu.SemaphoreType.DMA((16,)),
            pltpu.SemaphoreType.DMA((CHUNKS,)),
            pltpu.SemaphoreType.DMA((n_tp,)),
            pltpu.SemaphoreType.DMA((n_tp,)),
            pltpu.SemaphoreType.DMA,
            pltpu.SemaphoreType.DMA,
            pltpu.SemaphoreType.DMA((n_tp,)),
            pltpu.SemaphoreType.DMA((n_tp,)),
            pltpu.SemaphoreType.DMA,
            pltpu.SemaphoreType.DMA,
        ]

        def kernel(*refs):
            layer(n_ep, n_tp, *refs)

        return pl.pallas_call(
            kernel,
            name="layer",
            out_shape=jax.ShapeDtypeStruct((seqs, quarter), BF16),
            in_specs=specs,
            out_specs=pl.BlockSpec(memory_space=pltpu.VMEM),
            scratch_shapes=scratch,
            compiler_params=pltpu.CompilerParams(
                collective_id=0, has_side_effects=True, vmem_limit_bytes=66000000
            ),
        )(*args)

    return jax.shard_map(
        shards,
        mesh=mesh,
        in_specs=(
            P("ep", None),
            P("ep", None, "tp"),
            P("ep"),
            P(),
            P(None, "tp"),
            P(None, "tp"),
            P(None, "tp"),
            P("tp"),
            P(),
            P(),
            P(),
            P(None, "tp"),
            P(None, "tp"),
            P("tp", None),
            P(),
            P("ep", None),
            P(("ep", "tp"), None, None),
            P(("ep", "tp"), None, None),
            P(("ep", "tp"), None, None),
        ),
        out_specs=P("ep", "tp"),
        check_vma=False,
    )
```

time: 91.5 us -> 47.6 us (0.52)
  Pallas kernels: 0 us -> 37.6 us
  matrix products: 19.3 us -> 0 us
  blocking collectives: 18.9 us -> 0 us
  waiting for transfers between devices: 16.3 us -> 0 us
  starting transfers between devices: 11.9 us -> 0 us
  local copies, waits for them, and re-layouts: 19.3 us -> 8.42 us
  other arithmetic: 4.63 us -> 1.34 us
    pallas_call x0 -> x1, Pallas kernels: none -> 37.6 us  [shards(): pl.pallas_call(kernel, name='layer', out_shape=jax.ShapeDtypeStruct((seqs...]
    dot_general x13 -> x0, matrix products: 19.3 us -> none  [the longest x1 3.87 us: attention(): jnp.einsum('skgc,sckv->skgv', weight_old, values_old, preferred_element_t...]
    all_to_all x1 -> x0, blocking collectives: 18.9 us -> none  [shards(): lax.all_to_all(packed, 'ep', split_axis=0, concat_axis=0, tiled=True)]
    all_to_all x3 -> x0, waiting for transfers between devices: 16.3 us -> none  [the longest x1 8.62 us: shards(): lax.all_to_all(computed, 'ep', split_axis=0, concat_axis=0, tiled=True)]
    all_to_all x3 -> x0, starting transfers between devices: 11.9 us -> none  [the longest x1 4.83 us: sent_to_all(): return lax.all_to_all(copies, axis, split_axis=0, concat_axis=0, tiled=True)]
    unnamed x20 -> x5, local copies, waits for them, and re-layouts: 12.1 us -> 8.42 us
    reduce_sum x7 -> x0, other arithmetic: 3.4 us -> none  [the longest x1 1.7 us: attention(): totals = jnp.sum(expo_old, axis=-1) + expo_new]
    slice x1 -> x0, local copies, waits for them, and re-layouts: 2.65 us -> none  [attention(): layout[..., :v_width].reshape(seq_count, cache_len, kv_local, 2, qk_width)]
  transfers between devices with their start and end apart: 3 -> 0, of which waited for: 3 -> 0; matrix products, arithmetic and copies ran while one was open for 2% -> 0% of each run, Pallas kernels for 0% -> 0%
where the time goes in v1:
time: 47.6 us; the launch traced here: 47.3 us
  Pallas kernels  37.6 us (79%)
  local copies, waits for them, and re-layouts  8.42 us (18%)
  other arithmetic  1.34 us (3%)
    pallas_call x1, Pallas kernels, shards(): pl.pallas_call(kernel, name='layer', out_shape=jax.ShapeDtypeStruct((seqs...  37.6 us
    unnamed x5, local copies, waits for them, and re-layouts  8.42 us
    reshape x1, other arithmetic, shards(): gain2 = jnp.concatenate([head_gain, head_gain]).reshape(1, -1)  1.34 us

profile of v1, /device:TPU:1, one launch (start us, length us, event | category | flops | bytes accessed | tf_op | source)
XLA Modules:
  0.0 47.3 jit_solution(7949099926894546032)
XLA Ops:
  0.0 1.3 %maximum_bitcast_fusion.refs_8_ = f32[1,128]{1,0:T(1,128)} fusion(f32[64]{0:T(128)} %param.27), kind=kLoop, calls=%fused_computation | loop fusion | flops 128 | bytes 768 | tf_op jit(solution)/shard_map/reshape | solution.py:464
  1.3 1.4 %copy.23.refs_15_ = f32[32,4]{1,0:T(8,128)} copy(f32[32,4]{0,1:T(4,128)} %param.34) | data formatting | bytes 1024 | tf_op args[15]
  2.7 1.9 %copy.20.refs_5_ = bf16[2048,64]{1,0:T(8,128)(2,1)} copy(bf16[2048,64]{0,1:T(8,128)(2,1)} %param.24) | data formatting | bytes 524288 | tf_op args[5]
  4.7 2.0 %copy.21.refs_6_ = bf16[2048,64]{1,0:T(8,128)(2,1)} copy(bf16[2048,64]{0,1:T(8,128)(2,1)} %param.25) | data formatting | bytes 524288 | tf_op args[6]
  6.6 1.8 %copy.22.refs_14_ = s32[1024,4]{1,0:T(8,128)} copy(s32[1024,4]{0,1:T(4,128)} %param.33) | data formatting | bytes 32768 | tf_op args[14]
  8.4 37.6 %layer.1 = bf16[32,512]{1,0:T(8,128)(2,1)} custom-call(bf16[32,2048]{1,0:T(8,128)(2,1)} %refs_0_.1, bf16[32,1024,128]{2,1,0:T(8,128)(2,1)} %refs_1_.1, s32[32]{0:T(128)} %refs_2_.1, f32[1,2048]{1,0:T(1,128)} %bitcast.4, bf16[2048,256]{1,0:T(8,128)(2,1)} %refs_4_.1, bf16[2048,64]{1,0:T(8,128)(2,1)} %copy.20.refs_5_, bf16[2048,64]{1,0:T(8,128)(2,1)} %copy.21.refs_6_, ...), custom_call_target="tpu_custom_call" | custom-call | tf_op jit(solution)/shard_map/layer/pallas_call | solution.py:545
  45.9 1.4 %copy.25 = bf16[32,512]{1,0:T(8,128)(2,1)} copy(bf16[32,512]{1,0:T(8,128)(2,1)} %layer.1) | data formatting | bytes 65536

commit v2 on v1

--- a/solution.py
+++ b/solution.py
@@ -23,6 +23,17 @@
 
 def dot_ta(a, b):
     return lax.dot_general(a, b, (((0,), (0,)), ((), ())), preferred_element_type=F32)
+
+
+def dot_tb(a, b):
+    return lax.dot_general(a, b, (((1,), (1,)), ((), ())), preferred_element_type=F32)
+
+
+def turned(x):
+    tall, wide = x.shape
+    if wide < 128:
+        x = jnp.concatenate([x, jnp.zeros((tall, 128 - wide), F32)], axis=1)
+    return jnp.concatenate([x, jnp.zeros((128 - tall, 128), F32)], axis=0).T
 
 
 def layer(
@@ -52,8 +63,7 @@
     kv_v,
     attn_gain_v,
     wq_v,
-    wk_v,
-    wv_v,
+    wkv_v,
     head_gain_v,
     wo_v,
     ffn_gain_v,
@@ -62,6 +72,7 @@
     wsd_v,
     routing_v,
     rw_v,
+    table_v,
     wg_v,
     wu_v,
     wd_v,
@@ -69,7 +80,6 @@
     kvn_v,
     sc_v,
     wt_v,
-    acc_v,
     ho_v,
     proj_v,
     resid_v,
@@ -92,6 +102,7 @@
     sh_rs,
     r_ss,
     r_rs,
+    relay_sem,
 ):
     ep = lax.axis_index("ep")
     tp = lax.axis_index("tp")
@@ -108,9 +119,9 @@
         (tokens_h, tokens_v),
         (attn_gain_h, attn_gain_v),
         (wq_h, wq_v),
-        (wk_h, wk_v),
-        (wv_h, wv_v),
-        (routing_h.at[pl.ds(pl.multiple_of(ep * seqs, 8), seqs)], routing_v),
+        (wk_h, wkv_v.at[pl.ds(0, 64)]),
+        (wv_h, wkv_v.at[pl.ds(64, 64)]),
+        (routing_h.at[:, pl.ds(pl.multiple_of(lax.div(ep, 4) * 128, 128), 128)], routing_v),
         (rw_h, rw_v),
         (head_gain_h, head_gain_v),
         (ffn_gain_h, ffn_gain_v),
@@ -133,37 +144,38 @@
         )
     for copy in kv_copies:
         copy.start()
-    for copy in copies[9:]:
-        copy.start()
 
     barrier = pltpu.get_barrier_semaphore()
 
     def greet(d, carry):
-        other = lax.rem(me + d, n_dev)
         pl.semaphore_signal(
             barrier,
             inc=1,
-            device_id=(lax.div(other, n_tp), lax.rem(other, n_tp)),
+            device_id=(lax.rem(ep + d, n_ep), tp),
             device_id_type=MESH,
         )
         return carry
 
-    lax.fori_loop(1, n_dev, greet, 0)
+    lax.fori_loop(1, n_ep, greet, 0, unroll=True)
+    peers = [lax.rem(tp + d, n_tp) for d in range(n_tp)]
+    for d in range(1, n_tp):
+        pl.semaphore_signal(
+            barrier, inc=1, device_id=(ep, peers[d]), device_id_type=MESH
+        )
 
     qblk_v[...] = jnp.zeros_like(qblk_v)
 
     copies[0].wait()
     copies[1].wait()
+
     tok = tokens_v[...].astype(F32)
     mean = jnp.mean(tok * tok, axis=-1, keepdims=True)
     normed = (tok * lax.rsqrt(mean + EPS) * attn_gain_v[...]).astype(BF16)
     copies[2].wait()
     q = dot(normed, wq_v[...]).astype(BF16)
     copies[3].wait()
-    kn = dot(normed, wk_v[...])
     copies[4].wait()
-    vn = dot(normed, wv_v[...])
-    new_kv = jnp.concatenate([kn, vn], axis=1)
+    new_kv = dot_tb(normed, wkv_v[...])
 
     spread = (
         iota((seqs, heads * rows), 1)
@@ -190,12 +202,18 @@
     for h in range(heads):
         lam_lane = jnp.where(lane_head == h, lambdas_s[h], lam_lane)
 
-    lhs_new = jnp.concatenate([kvn_v[s] for s in range(seqs)], axis=1)
-    sc_new = dot(lhs_new, qblk_v[...])
-    sc_new = jnp.where(iota((16, 2 * rows), 0) == 0, sc_new, NEG)
-    top = jnp.max(sc_new, axis=0, keepdims=True)
+    top = jnp.full((1, 2 * rows), NEG, F32)
     for c in range(CHUNKS):
-        kv_copies[c].wait()
+        if c % 2 == 0:
+            kv_copies[c].wait()
+            kv_copies[c + 1].wait()
+        if c == 2:
+            for copy in copies[9:]:
+                copy.start()
+            lhs_new = jnp.concatenate([kvn_v[s] for s in range(seqs)], axis=1)
+            sc_new = dot(lhs_new, qblk_v[...])
+            sc_new = jnp.where(iota((16, 2 * rows), 0) == 0, sc_new, NEG)
+            top = jnp.maximum(top, jnp.max(sc_new, axis=0, keepdims=True))
         part = pl.ds(c * chunk, chunk)
         lhs = jnp.concatenate([kv_v[s, part, :] for s in range(seqs)], axis=1)
         sc = dot(lhs, qblk_v[...])
@@ -222,27 +240,21 @@
         w = sc_v[part, 0:rows] * inv1 - sc_v[part, rows : 2 * rows] * inv2
         wt_v[:, part] = w.T.astype(BF16)
 
-    acc_v[...] = jnp.zeros_like(acc_v)
+    acc = jnp.zeros((rows, 128), F32)
     row_seq = lax.rem(iota((rows, 128), 0), seqs)
-
-    def mix(p, carry):
-        base = p * 4
+    for base in range(0, seqs, 4):
         rhs = jnp.concatenate([kv_v[base + i] for i in range(4)], axis=1)
         rhs_new = jnp.concatenate([kvn_v[base + i] for i in range(4)], axis=1)
         o = dot(wt_v[...], rhs) + dot(wt_new[:, 0:16], rhs_new)
-        acc = acc_v[...]
         for i in range(4):
             acc = jnp.where(row_seq == base + i, o[:, i * 128 : (i + 1) * 128], acc)
-        acc_v[...] = acc
-        return carry
-
-    lax.fori_loop(0, seqs // 4, mix, 0)
 
     upper = iota((rows, 128), 1) >= 64
-    mixv = jnp.where(upper, acc_v[...], 0.0)
+    mixv = jnp.where(upper, acc, 0.0)
     copies[7].wait()
     ms = jnp.sum(mixv * mixv, axis=-1, keepdims=True) * (1.0 / 64.0)
-    ho = mixv * lax.rsqrt(ms + EPS) * head_gain_v[...]
+    gain = head_gain_v[...]
+    ho = mixv * lax.rsqrt(ms + EPS) * jnp.concatenate([gain, gain], axis=1)
     low = iota((seqs, 128), 1) < 64
     halves = []
     for i in range(2):
@@ -252,7 +264,7 @@
     head_out = jnp.concatenate(halves, axis=1).astype(BF16)
     ho_v[tp] = head_out
 
-    pl.semaphore_wait(barrier, n_dev - 1)
+    pl.semaphore_wait(barrier, n_ep + n_tp - 2)
     ho_copies = []
     for d in range(1, n_tp):
         copy = pltpu.make_async_remote_copy(
@@ -260,16 +272,23 @@
             dst_ref=ho_v.at[tp],
             send_sem=ho_ss.at[d],
             recv_sem=ho_rs.at[d],
-            device_id=(ep, lax.rem(tp + d, n_tp)),
+            device_id=(ep, peers[d]),
             device_id_type=MESH,
         )
         copy.start()
         ho_copies.append(copy)
+    for d in range(1, n_tp):
+        pl.semaphore_signal(
+            relay_sem, inc=1, device_id=(ep, peers[d]), device_id_type=MESH
+        )
 
     copies[5].wait()
     copies[6].wait()
     e_lane = iota((seqs, n_dev), 1)
-    picks = [routing_v[:, k : k + 1] for k in range(4)]
+    table_v[...] = turned(routing_v[...].astype(F32))
+    own = table_v[pl.ds(pl.multiple_of(lax.rem(ep, 4) * seqs, 8), seqs), :]
+    picks = [own[:, k : k + 1].astype(jnp.int32) for k in range(4)]
+    rw = turned(rw_v[...])[0:seqs]
     hots = [(e_lane == r).astype(F32) for r in picks]
     named = hots[0] + hots[1] + hots[2] + hots[3]
     earlier = (iota((seqs, seqs), 1) < iota((seqs, seqs), 0)).astype(BF16)
@@ -290,7 +309,7 @@
         piece = jnp.zeros((seqs, n_dev * 8), F32)
         for k in range(4):
             slot = picks[k] * 8 + ranks[k] * 4 + b
-            piece = jnp.where(m_col == slot, rw_v[:, k : k + 1], piece)
+            piece = jnp.where(m_col == slot, rw[:, k : k + 1], piece)
         high = piece.astype(BF16)
         m2_v[b * seqs : (b + 1) * seqs, :] = high
         m2_v[(4 + b) * seqs : (5 + b) * seqs, :] = (piece - high.astype(F32)).astype(BF16)
@@ -394,9 +413,9 @@
         send2_v[:, t] = back[:, t * 128 : (t + 1) * 128].reshape(n_ep, 8, 128)
     recv2_v[me] = send2_v[ep, tp]
 
-    def give_back(d, carry):
-        other = lax.rem(me + d, n_dev)
-        oe, ot = lax.div(other, n_tp), lax.rem(other, n_tp)
+    pl.semaphore_wait(relay_sem, n_tp - 1)
+
+    def give(oe, ot):
         pltpu.make_async_remote_copy(
             src_ref=send2_v.at[oe, ot],
             dst_ref=recv2_v.at[me],
@@ -405,9 +424,16 @@
             device_id=(oe, ot),
             device_id_type=MESH,
         ).start()
+
+    def give_back(d, carry):
+        oe = lax.rem(ep + d, n_ep)
+        for ot in peers:
+            give(oe, ot)
         return carry
 
-    lax.fori_loop(1, n_dev, give_back, 0)
+    lax.fori_loop(1, n_ep, give_back, 0)
+    for ot in peers[1:]:
+        give(ep, ot)
 
     final = resid_v[tp].astype(F32) + shs_v[tp].astype(F32)
     for copy in sh_copies:
@@ -461,29 +487,28 @@
         n_dev = n_ep * n_tp
         quarter = width // n_tp
         rows = 4 * seqs
-        gain2 = jnp.concatenate([head_gain, head_gain]).reshape(1, -1)
         args = (
             tokens,
             kv_cache,
             lengths,
             attn_gain.reshape(1, -1),
             w_query,
-            w_key,
-            w_value,
+            w_key.T,
+            w_value.T,
             lambdas,
-            gain2,
+            head_gain.reshape(1, -1),
             w_out,
             ffn_gain.reshape(1, -1),
             w_shared_gate,
             w_shared_up,
             w_shared_down,
-            routing,
-            route_weights,
+            routing.T,
+            route_weights.T,
             w_exp_gate,
             w_exp_up,
             w_exp_down,
         )
-        anyspec = pl.BlockSpec(memory_space=pl.ANY)
+        anyspec = pl.BlockSpec(memory_space=pltpu.HBM)
         smem = pl.BlockSpec(memory_space=pltpu.SMEM)
         specs = [anyspec] * len(args)
         specs[2] = smem
@@ -497,16 +522,16 @@
             vm(kv_cache),
             pltpu.VMEM((1, width), F32),
             vm(w_query),
-            vm(w_key),
-            vm(w_value),
-            pltpu.VMEM((1, 128), F32),
+            pltpu.VMEM((128, width), BF16),
+            pltpu.VMEM((1, 64), F32),
             vm(w_out),
             pltpu.VMEM((1, width), F32),
             vm(w_shared_gate),
             vm(w_shared_up),
             vm(w_shared_down),
-            pltpu.VMEM((seqs, 4), jnp.int32),
-            vm(route_weights),
+            pltpu.VMEM((4, 128), jnp.int32),
+            pltpu.VMEM((4, seqs), F32),
+            pltpu.VMEM((128, 128), F32),
             pltpu.VMEM(w_exp_gate.shape[1:], BF16),
             pltpu.VMEM(w_exp_up.shape[1:], BF16),
             pltpu.VMEM(w_exp_down.shape[1:], BF16),
@@ -514,7 +539,6 @@
             pltpu.VMEM((seqs, 16, 128), BF16),
             pltpu.VMEM((kv_cache.shape[1], 2 * rows), F32),
             pltpu.VMEM((rows, kv_cache.shape[1]), BF16),
-            pltpu.VMEM((rows, 128), F32),
             pltpu.VMEM((n_tp, seqs, 256), BF16),
             pltpu.VMEM((seqs, width), F32),
             pltpu.VMEM((n_tp, seqs, quarter), BF16),
@@ -537,6 +561,7 @@
             pltpu.SemaphoreType.DMA((n_tp,)),
             pltpu.SemaphoreType.DMA,
             pltpu.SemaphoreType.DMA,
+            pltpu.SemaphoreType.REGULAR,
         ]
 
         def kernel(*refs):
@@ -550,7 +575,7 @@
             out_specs=pl.BlockSpec(memory_space=pltpu.VMEM),
             scratch_shapes=scratch,
             compiler_params=pltpu.CompilerParams(
-                collective_id=0, has_side_effects=True, vmem_limit_bytes=66000000
+                collective_id=0, has_side_effects=True, vmem_limit_bytes=64000000
             ),
         )(*args)
 

time: 47.6 us -> 34.9 us (0.73)
  local copies, waits for them, and re-layouts: 8.42 us -> 1.38 us
  Pallas kernels: 37.6 us -> 33.3 us
  other arithmetic: 1.34 us -> 0 us
    unnamed x5 -> x1, local copies, waits for them, and re-layouts: 8.42 us -> 1.38 us
    pallas_call x1, Pallas kernels: 37.6 us -> 33.3 us  [shards(): pl.pallas_call(kernel, name='layer', out_shape=jax.ShapeDtypeStruct((seqs...]
    reshape x1 -> x0, other arithmetic: 1.34 us -> none  [shards(): gain2 = jnp.concatenate([head_gain, head_gain]).reshape(1, -1)]
where the time goes in v2:
time: 34.9 us; the launch traced here: 34.7 us
  Pallas kernels  33.3 us (95%)
  local copies, waits for them, and re-layouts  1.38 us (4%)
    pallas_call x1, Pallas kernels, shards(): pl.pallas_call(kernel, name='layer', out_shape=jax.ShapeDtypeStruct((seqs...  33.3 us
    unnamed x1, local copies, waits for them, and re-layouts  1.38 us

profile of v2, /device:TPU:1, one launch (start us, length us, event | category | flops | bytes accessed | tf_op | source)
XLA Modules:
  0.0 34.7 jit_solution(4263100899273546780)
XLA Ops:
  0.0 33.3 %layer.1 = bf16[32,512]{1,0:T(8,128)(2,1)} custom-call(bf16[32,2048]{1,0:T(8,128)(2,1)} %refs_0_.1, bf16[32,1024,128]{2,1,0:T(8,128)(2,1)} %refs_1_.1, s32[32]{0:T(128)} %refs_2_.1, f32[1,2048]{1,0:T(1,128)} %bitcast.10, bf16[2048,256]{1,0:T(8,128)(2,1)} %refs_4_.1, bf16[64,2048]{1,0:T(8,128)(2,1)} %bitcast.7, bf16[64,2048]{1,0:T(8,128)(2,1)} %bitcast.8, ...), custom_call_target="tpu_custom_call" | custom-call | tf_op jit(solution)/shard_map/layer/pallas_call | solution.py:570
  33.3 1.4 %copy.21 = bf16[32,512]{1,0:T(8,128)(2,1)} copy(bf16[32,512]{1,0:T(8,128)(2,1)} %layer.1) | data formatting | bytes 65536

commit v3 on v2

--- a/solution.py
+++ b/solution.py
@@ -34,6 +34,10 @@
     if wide < 128:
         x = jnp.concatenate([x, jnp.zeros((tall, 128 - wide), F32)], axis=1)
     return jnp.concatenate([x, jnp.zeros((128 - tall, 128), F32)], axis=0).T
+
+
+def hops(d, n):
+    return min(d, n - d)
 
 
 def layer(
@@ -114,6 +118,32 @@
     heads = 4
     qk = 32
     rows = heads * seqs
+    pairs = seqs // 2
+
+    peers = [lax.rem(tp + d, n_tp) for d in range(n_tp)]
+    ez, ey, ec = lax.div(ep, 8), lax.rem(lax.div(ep, 2), 4), lax.rem(ep, 2)
+    zs = [lax.rem(ez + d, 4) * 8 for d in range(4)]
+    ys = [lax.rem(ey + d, 4) * 2 for d in range(4)]
+    cs = [ec, 1 - ec]
+    far_peers = sorted(
+        (
+            (zs[dz] + ys[dy] + cs[dc], hops(dz, 4) + hops(dy, 4))
+            for dz in range(4)
+            for dy in range(4)
+            for dc in range(2)
+            if dz + dy + dc
+        ),
+        key=lambda p: -p[1],
+    )
+    far_all = sorted(
+        (
+            (h + hops(d, n_tp), oe, d)
+            for oe, h in far_peers + [(ep, 0)]
+            for d in range(n_tp)
+            if h + d or oe is not ep
+        ),
+        key=lambda p: -p[0],
+    )
 
     order = [
         (tokens_h, tokens_v),
@@ -147,17 +177,10 @@
 
     barrier = pltpu.get_barrier_semaphore()
 
-    def greet(d, carry):
+    for other, _ in far_peers:
         pl.semaphore_signal(
-            barrier,
-            inc=1,
-            device_id=(lax.rem(ep + d, n_ep), tp),
-            device_id_type=MESH,
-        )
-        return carry
-
-    lax.fori_loop(1, n_ep, greet, 0, unroll=True)
-    peers = [lax.rem(tp + d, n_tp) for d in range(n_tp)]
+            barrier, inc=1, device_id=(other, tp), device_id_type=MESH
+        )
     for d in range(1, n_tp):
         pl.semaphore_signal(
             barrier, inc=1, device_id=(ep, peers[d]), device_id_type=MESH
@@ -189,9 +212,21 @@
     lane_seq = lax.rem(iota((2 * qk, rows), 1), seqs)
     for s in range(seqs):
         block = jnp.where(lane_seq == s, qt, 0.0).astype(BF16)
-        qblk_v[s * 128 : s * 128 + qk, 0:rows] = block[0:qk]
-        qblk_v[s * 128 + qk : s * 128 + 2 * qk, rows : 2 * rows] = block[qk : 2 * qk]
-        kvn_v[s] = jnp.broadcast_to(new_kv[s : s + 1, :], (16, 128)).astype(BF16)
+        base = s * 2 * qk
+        qblk_v[base : base + qk, 0:rows] = block[0:qk]
+        qblk_v[base + qk : base + 2 * qk, rows : 2 * rows] = block[qk : 2 * qk]
+    low_new = iota((seqs, 128), 1) < 64
+    turned_new = pltpu.roll(new_kv, 64, 1)
+    k_new = jnp.where(low_new, new_kv, turned_new)
+    v_new = jnp.where(low_new, turned_new, new_kv)
+    low16 = iota((16, 128), 1) < 64
+    for p in range(pairs):
+        for i, new in enumerate((k_new, v_new)):
+            kvn_v[i, p] = jnp.where(
+                low16,
+                jnp.broadcast_to(new[2 * p : 2 * p + 1, :], (16, 128)),
+                jnp.broadcast_to(new[2 * p + 1 : 2 * p + 2, :], (16, 128)),
+            ).astype(BF16)
 
     lane1 = iota((1, 2 * rows), 1)
     len_lane = jnp.zeros((1, 2 * rows), jnp.int32)
@@ -203,24 +238,34 @@
         lam_lane = jnp.where(lane_head == h, lambdas_s[h], lam_lane)
 
     top = jnp.full((1, 2 * rows), NEG, F32)
+    part_rows = chunk // 2
+    low = iota((part_rows, 128), 1) < 64
     for c in range(CHUNKS):
-        if c % 2 == 0:
-            kv_copies[c].wait()
-            kv_copies[c + 1].wait()
-        if c == 2:
+        kv_copies[c].wait()
+        if c == CHUNKS - 1:
             for copy in copies[9:]:
                 copy.start()
-            lhs_new = jnp.concatenate([kvn_v[s] for s in range(seqs)], axis=1)
+            lhs_new = jnp.concatenate([kvn_v[0, p] for p in range(pairs)], axis=1)
             sc_new = dot(lhs_new, qblk_v[...])
             sc_new = jnp.where(iota((16, 2 * rows), 0) == 0, sc_new, NEG)
             top = jnp.maximum(top, jnp.max(sc_new, axis=0, keepdims=True))
-        part = pl.ds(c * chunk, chunk)
-        lhs = jnp.concatenate([kv_v[s, part, :] for s in range(seqs)], axis=1)
-        sc = dot(lhs, qblk_v[...])
-        valid = iota((chunk, 2 * rows), 0) + c * chunk < len_lane
-        sc = jnp.where(valid, sc, NEG)
-        sc_v[part, :] = sc
-        top = jnp.maximum(top, jnp.max(sc, axis=0, keepdims=True))
+        for i in range(2):
+            start = c * chunk + i * part_rows
+            part = pl.ds(start, part_rows)
+            lhs = jnp.concatenate(
+                [
+                    jnp.where(
+                        low, kv_v[2 * p, part, :], pltpu.roll(kv_v[2 * p + 1, part, :], 64, 1)
+                    )
+                    for p in range(pairs)
+                ],
+                axis=1,
+            )
+            sc = dot(lhs, qblk_v[...])
+            valid = iota((part_rows, 2 * rows), 0) + start < len_lane
+            sc = jnp.where(valid, sc, NEG)
+            sc_v[part, :] = sc
+            top = jnp.maximum(top, jnp.max(sc, axis=0, keepdims=True))
 
     scaling = qk ** (-0.5)
     ex_new = jnp.exp((sc_new - top) * scaling)
@@ -241,32 +286,40 @@
         wt_v[:, part] = w.T.astype(BF16)
 
     acc = jnp.zeros((rows, 128), F32)
-    row_seq = lax.rem(iota((rows, 128), 0), seqs)
-    for base in range(0, seqs, 4):
-        rhs = jnp.concatenate([kv_v[base + i] for i in range(4)], axis=1)
-        rhs_new = jnp.concatenate([kvn_v[base + i] for i in range(4)], axis=1)
+    row_pair = lax.rem(iota((rows, 128), 0), seqs) // 2
+    low = iota((cache, 128), 1) < 64
+    for base in range(0, pairs, 4):
+        rhs = jnp.concatenate(
+            [
+                jnp.where(low, pltpu.roll(kv_v[2 * p], 64, 1), kv_v[2 * p + 1])
+                for p in range(base, base + 4)
+            ],
+            axis=1,
+        )
+        rhs_new = jnp.concatenate([kvn_v[1, p] for p in range(base, base + 4)], axis=1)
         o = dot(wt_v[...], rhs) + dot(wt_new[:, 0:16], rhs_new)
         for i in range(4):
-            acc = jnp.where(row_seq == base + i, o[:, i * 128 : (i + 1) * 128], acc)
-
-    upper = iota((rows, 128), 1) >= 64
-    mixv = jnp.where(upper, acc, 0.0)
+            acc = jnp.where(row_pair == base + i, o[:, i * 128 : (i + 1) * 128], acc)
+
+    odd = lax.rem(iota((rows, 128), 0), 2) == 1
+    mixv = jnp.where(odd == (iota((rows, 128), 1) >= 64), acc, 0.0)
     copies[7].wait()
     ms = jnp.sum(mixv * mixv, axis=-1, keepdims=True) * (1.0 / 64.0)
     gain = head_gain_v[...]
+    mixv = mixv + pltpu.roll(mixv, 64, 1)
     ho = mixv * lax.rsqrt(ms + EPS) * jnp.concatenate([gain, gain], axis=1)
     low = iota((seqs, 128), 1) < 64
     halves = []
     for i in range(2):
         even = ho[(2 * i) * seqs : (2 * i + 1) * seqs]
         odd = ho[(2 * i + 1) * seqs : (2 * i + 2) * seqs]
-        halves.append(jnp.where(low, pltpu.roll(even, 64, 1), odd))
+        halves.append(jnp.where(low, even, odd))
     head_out = jnp.concatenate(halves, axis=1).astype(BF16)
     ho_v[tp] = head_out
 
     pl.semaphore_wait(barrier, n_ep + n_tp - 2)
-    ho_copies = []
-    for d in range(1, n_tp):
+    ho_copies = {}
+    for d in (2, 1, 3):
         copy = pltpu.make_async_remote_copy(
             src_ref=ho_v.at[tp],
             dst_ref=ho_v.at[tp],
@@ -276,7 +329,7 @@
             device_id_type=MESH,
         )
         copy.start()
-        ho_copies.append(copy)
+        ho_copies[d] = copy
     for d in range(1, n_tp):
         pl.semaphore_signal(
             relay_sem, inc=1, device_id=(ep, peers[d]), device_id_type=MESH
@@ -327,7 +380,7 @@
 
     proj_v[...] = project(tp)
     for d in (1, 3, 2):
-        ho_copies[d - 1].wait_recv()
+        ho_copies[d].wait_recv()
         owner = lax.rem(tp + n_tp - d, n_tp)
         proj_v[...] += project(owner)
     copies[8].wait()
@@ -346,8 +399,7 @@
     send1_v[...] = packed.reshape(send1_v.shape)
     recv1_v[ep] = send1_v[ep]
 
-    def dispatch(d, carry):
-        other = lax.rem(ep + d, n_ep)
+    for other, _ in far_peers:
         pltpu.make_async_remote_copy(
             src_ref=send1_v.at[other],
             dst_ref=recv1_v.at[ep],
@@ -356,9 +408,6 @@
             device_id=(other, tp),
             device_id_type=MESH,
         ).start()
-        return carry
-
-    lax.fori_loop(1, n_ep, dispatch, 0)
 
     copies[10].wait()
     copies[11].wait()
@@ -425,15 +474,8 @@
             device_id_type=MESH,
         ).start()
 
-    def give_back(d, carry):
-        oe = lax.rem(ep + d, n_ep)
-        for ot in peers:
-            give(oe, ot)
-        return carry
-
-    lax.fori_loop(1, n_ep, give_back, 0)
-    for ot in peers[1:]:
-        give(ep, ot)
+    for _, oe, d in far_all:
+        give(oe, peers[d])
 
     final = resid_v[tp].astype(F32) + shs_v[tp].astype(F32)
     for copy in sh_copies:
@@ -450,7 +492,7 @@
     )
     out_ref[...] = final.astype(BF16)
 
-    for copy in ho_copies:
+    for copy in ho_copies.values():
         copy.wait_send()
     for copy in sh_copies:
         copy.wait_send()
@@ -535,8 +577,8 @@
             pltpu.VMEM(w_exp_gate.shape[1:], BF16),
             pltpu.VMEM(w_exp_up.shape[1:], BF16),
             pltpu.VMEM(w_exp_down.shape[1:], BF16),
-            pltpu.VMEM((seqs * 128, 2 * rows), BF16),
-            pltpu.VMEM((seqs, 16, 128), BF16),
+            pltpu.VMEM((seqs * 64, 2 * rows), BF16),
+            pltpu.VMEM((2, seqs // 2, 16, 128), BF16),
             pltpu.VMEM((kv_cache.shape[1], 2 * rows), F32),
             pltpu.VMEM((rows, kv_cache.shape[1]), BF16),
             pltpu.VMEM((n_tp, seqs, 256), BF16),

time: 34.9 us -> 32.8 us (0.940)
  Pallas kernels: 33.3 us -> 31.3 us
    pallas_call x1, Pallas kernels: 33.3 us -> 31.3 us  [shards(): pl.pallas_call(kernel, name='layer', out_shape=jax.ShapeDtypeStruct((seqs...]
where the time goes in v3:
time: 32.8 us; the launch traced here: 32.7 us
  Pallas kernels  31.3 us (95%)
  local copies, waits for them, and re-layouts  1.38 us (4%)
    pallas_call x1, Pallas kernels, shards(): pl.pallas_call(kernel, name='layer', out_shape=jax.ShapeDtypeStruct((seqs...  31.3 us
    unnamed x1, local copies, waits for them, and re-layouts  1.38 us

profile of v3, /device:TPU:1, one launch (start us, length us, event | category | flops | bytes accessed | tf_op | source)
XLA Modules:
  0.0 32.7 jit_solution(5027623536788798150)
XLA Ops:
  0.0 31.3 %layer.1 = bf16[32,512]{1,0:T(8,128)(2,1)} custom-call(bf16[32,2048]{1,0:T(8,128)(2,1)} %refs_0_.1, bf16[32,1024,128]{2,1,0:T(8,128)(2,1)} %refs_1_.1, s32[32]{0:T(128)} %refs_2_.1, f32[1,2048]{1,0:T(1,128)} %bitcast.10, bf16[2048,256]{1,0:T(8,128)(2,1)} %refs_4_.1, bf16[64,2048]{1,0:T(8,128)(2,1)} %bitcast.7, bf16[64,2048]{1,0:T(8,128)(2,1)} %bitcast.8, ...), custom_call_target="tpu_custom_call" | custom-call | tf_op jit(solution)/shard_map/layer/pallas_call | solution.py:612
  31.3 1.4 %copy.21 = bf16[32,512]{1,0:T(8,128)(2,1)} copy(bf16[32,512]{1,0:T(8,128)(2,1)} %layer.1) | data formatting | bytes 65536

commit v4 on v3

--- a/solution.py
+++ b/solution.py
@@ -88,6 +88,11 @@
     proj_v,
     resid_v,
     oh_v,
+    ohh_v,
+    xbig_v,
+    sendh_v,
+    recvh_v,
+    tok_v,
     fold_v,
     m2_v,
     send1_v,
@@ -106,6 +111,8 @@
     sh_rs,
     r_ss,
     r_rs,
+    h_ss,
+    h_rs,
     relay_sem,
 ):
     ep = lax.axis_index("ep")
@@ -127,45 +134,49 @@
     cs = [ec, 1 - ec]
     far_peers = sorted(
         (
-            (zs[dz] + ys[dy] + cs[dc], hops(dz, 4) + hops(dy, 4))
+            (-hops(dz, 4) - hops(dy, 4), dc, (dz * 7 + dy * 5) % 11, zs[dz] + ys[dy] + cs[dc])
             for dz in range(4)
             for dy in range(4)
             for dc in range(2)
             if dz + dy + dc
         ),
-        key=lambda p: -p[1],
+        key=lambda p: p[:3],
     )
     far_all = sorted(
-        (
-            (h + hops(d, n_tp), oe, d)
-            for oe, h in far_peers + [(ep, 0)]
-            for d in range(n_tp)
-            if h + d or oe is not ep
+        [(p[0] - hops(d, n_tp), p[1], p[2], d, p[3]) for p in far_peers for d in range(n_tp)]
+        + [(-hops(d, n_tp), 0, 0, d, ep) for d in range(1, n_tp)],
+        key=lambda p: p[:4],
+    )
+
+    order = {
+        "routing": (
+            routing_h.at[:, pl.ds(pl.multiple_of(lax.div(ep, 4) * 128, 128), 128)],
+            routing_v,
         ),
-        key=lambda p: -p[0],
-    )
-
-    order = [
-        (tokens_h, tokens_v),
-        (attn_gain_h, attn_gain_v),
-        (wq_h, wq_v),
-        (wk_h, wkv_v.at[pl.ds(0, 64)]),
-        (wv_h, wkv_v.at[pl.ds(64, 64)]),
-        (routing_h.at[:, pl.ds(pl.multiple_of(lax.div(ep, 4) * 128, 128), 128)], routing_v),
-        (rw_h, rw_v),
-        (head_gain_h, head_gain_v),
-        (ffn_gain_h, ffn_gain_v),
-        (wo_h, wo_v),
-        (wsg_h, wsg_v),
-        (wsu_h, wsu_v),
-        (wsd_h, wsd_v),
-        (wg_h.at[0], wg_v),
-        (wu_h.at[0], wu_v),
-        (wd_h.at[0], wd_v),
-    ]
-    copies = [pltpu.make_async_copy(a, b, lsem.at[i]) for i, (a, b) in enumerate(order)]
-    for copy in copies[:9]:
-        copy.start()
+        "tokens": (tokens_h, tokens_v),
+        "attn_gain": (attn_gain_h, attn_gain_v),
+        "wq": (wq_h, wq_v),
+        "wk": (wk_h, wkv_v.at[pl.ds(0, 64)]),
+        "wv": (wv_h, wkv_v.at[pl.ds(64, 64)]),
+        "rw": (rw_h, rw_v),
+        "head_gain": (head_gain_h, head_gain_v),
+        "ffn_gain": (ffn_gain_h, ffn_gain_v),
+        "wo": (wo_h, wo_v),
+        "wsg": (wsg_h, wsg_v),
+        "wsu": (wsu_h, wsu_v),
+        "wsd": (wsd_h, wsd_v),
+        "wg": (wg_h.at[0], wg_v),
+        "wu": (wu_h.at[0], wu_v),
+        "wd": (wd_h.at[0], wd_v),
+    }
+    copies = {
+        name: pltpu.make_async_copy(a, b, lsem.at[i])
+        for i, (name, (a, b)) in enumerate(order.items())
+    }
+    late = ("wo", "wsg", "wsu", "wsd", "wg", "wu", "wd")
+    for name, copy in copies.items():
+        if name not in late:
+            copy.start()
     kv_copies = []
     for c in range(CHUNKS):
         part = pl.ds(c * chunk, chunk)
@@ -177,7 +188,7 @@
 
     barrier = pltpu.get_barrier_semaphore()
 
-    for other, _ in far_peers:
+    for *_, other in far_peers:
         pl.semaphore_signal(
             barrier, inc=1, device_id=(other, tp), device_id_type=MESH
         )
@@ -187,17 +198,55 @@
         )
 
     qblk_v[...] = jnp.zeros_like(qblk_v)
-
-    copies[0].wait()
-    copies[1].wait()
+    xbig_v[...] = jnp.zeros_like(xbig_v)
+
+    copies["tokens"].wait()
+    copies["attn_gain"].wait()
 
     tok = tokens_v[...].astype(F32)
     mean = jnp.mean(tok * tok, axis=-1, keepdims=True)
     normed = (tok * lax.rsqrt(mean + EPS) * attn_gain_v[...]).astype(BF16)
-    copies[2].wait()
+    copies["routing"].wait()
+    block = routing_v[...].astype(F32)
+    table_v[...] = turned(block)
+    own = table_v[pl.ds(pl.multiple_of(lax.rem(ep, 4) * seqs, 8), seqs), :]
+    picks = [own[:, k : k + 1].astype(jnp.int32) for k in range(4)]
+    lane4 = iota((4, 128), 1)
+    row4 = pltpu.roll(block, lax.rem(4 - lax.rem(ep, 4), 4) * seqs, 1)
+    row4 = jnp.where(lane4 < seqs, row4, 0.0)
+    row4 = row4 + pltpu.roll(row4, seqs, 1)
+    row4 = (row4 + pltpu.roll(row4, 2 * seqs, 1)).astype(jnp.int32)
+    sub = iota((seqs, 128), 0)
+    before_lane = sub < lax.rem(iota((seqs, 128), 1), seqs)
+    slots, columns = [], []
+    for k in range(4):
+        row = row4[k : k + 1, :]
+        same = jnp.zeros((seqs, 128), F32)
+        for j in range(4):
+            same = same + (picks[j] == row).astype(F32)
+        rank = jnp.sum(jnp.where(before_lane, same, 0.0), axis=0, keepdims=True)
+        slots.append((row // n_tp) * 8 + rank.astype(jnp.int32) * 4)
+        columns.append(lax.rem(row, n_tp))
+    lane1 = iota((1, 128), 1)
+    slot_row = iota((n_ep * 8, 128), 0)
+
+    def slot_table(column, a):
+        hit = jnp.zeros((n_ep * 8, 128), F32)
+        for k in range(4):
+            at = jnp.where(columns[k] == column, slots[k] + a, -1)
+            hit = jnp.where(slot_row == at, 1.0, hit)
+        return hit.astype(BF16)
+
+    oh_v[...] = slot_table(tp, lane1 // seqs)
+    for i in range(2):
+        ohh_v[:, i * 128 : (i + 1) * 128] = slot_table(
+            2 * i + lane1 // 64, lax.rem(lane1 // seqs, 2)
+        )
+
+    copies["wq"].wait()
+    copies["wk"].wait()
+    copies["wv"].wait()
     q = dot(normed, wq_v[...]).astype(BF16)
-    copies[3].wait()
-    copies[4].wait()
     new_kv = dot_tb(normed, wkv_v[...])
 
     spread = (
@@ -237,14 +286,36 @@
     for h in range(heads):
         lam_lane = jnp.where(lane_head == h, lambdas_s[h], lam_lane)
 
+    quarter = width // n_tp
+    folded = jnp.concatenate(
+        [tokens_v[:, a * quarter : (a + 1) * quarter] for a in range(4)], axis=0
+    )
+    send1_v[...] = dot(oh_v[...], folded).astype(BF16).reshape(send1_v.shape)
+    recv1_v[ep] = send1_v[ep]
+
     top = jnp.full((1, 2 * rows), NEG, F32)
     part_rows = chunk // 2
     low = iota((part_rows, 128), 1) < 64
     for c in range(CHUNKS):
+        if c == CHUNKS // 2:
+            pl.semaphore_wait(barrier, n_ep + n_tp - 2)
+            for d in range(1, n_tp):
+                pl.semaphore_signal(relay_sem, inc=1, device_id=(ep, peers[d]), device_id_type=MESH)
+            for *_, other in far_peers:
+                pltpu.make_async_remote_copy(
+                    src_ref=send1_v.at[other],
+                    dst_ref=recv1_v.at[ep],
+                    send_sem=d_ss,
+                    recv_sem=d_rs,
+                    device_id=(other, tp),
+                    device_id_type=MESH,
+                ).start()
         kv_copies[c].wait()
         if c == CHUNKS - 1:
-            for copy in copies[9:]:
-                copy.start()
+            for name in ("rw", "head_gain", "ffn_gain"):
+                copies[name].wait()
+            for name in late:
+                copies[name].start()
             lhs_new = jnp.concatenate([kvn_v[0, p] for p in range(pairs)], axis=1)
             sc_new = dot(lhs_new, qblk_v[...])
             sc_new = jnp.where(iota((16, 2 * rows), 0) == 0, sc_new, NEG)
@@ -303,7 +374,6 @@
 
     odd = lax.rem(iota((rows, 128), 0), 2) == 1
     mixv = jnp.where(odd == (iota((rows, 128), 1) >= 64), acc, 0.0)
-    copies[7].wait()
     ms = jnp.sum(mixv * mixv, axis=-1, keepdims=True) * (1.0 / 64.0)
     gain = head_gain_v[...]
     mixv = mixv + pltpu.roll(mixv, 64, 1)
@@ -316,8 +386,18 @@
         halves.append(jnp.where(low, even, odd))
     head_out = jnp.concatenate(halves, axis=1).astype(BF16)
     ho_v[tp] = head_out
-
-    pl.semaphore_wait(barrier, n_ep + n_tp - 2)
+    for t in range(n_tp):
+        for a in range(2):
+            row = (2 * t + a) * seqs
+            xbig_v[row : row + seqs, t * 128 : (t + 1) * 128] = head_out[
+                :, a * 128 : (a + 1) * 128
+            ]
+    packed = dot(ohh_v[...], xbig_v[...]).astype(BF16)
+    for t in range(n_tp):
+        sendh_v[:, t] = packed[:, t * 128 : (t + 1) * 128].reshape(n_ep, 8, 128)
+    recvh_v[tp * n_ep + ep] = sendh_v[ep, tp]
+
+    pl.semaphore_wait(relay_sem, n_tp - 1)
     ho_copies = {}
     for d in (2, 1, 3):
         copy = pltpu.make_async_remote_copy(
@@ -330,33 +410,24 @@
         )
         copy.start()
         ho_copies[d] = copy
-    for d in range(1, n_tp):
-        pl.semaphore_signal(
-            relay_sem, inc=1, device_id=(ep, peers[d]), device_id_type=MESH
-        )
-
-    copies[5].wait()
-    copies[6].wait()
-    e_lane = iota((seqs, n_dev), 1)
-    table_v[...] = turned(routing_v[...].astype(F32))
-    own = table_v[pl.ds(pl.multiple_of(lax.rem(ep, 4) * seqs, 8), seqs), :]
-    picks = [own[:, k : k + 1].astype(jnp.int32) for k in range(4)]
+    for *_, d, oe in far_all:
+        pltpu.make_async_remote_copy(
+            src_ref=sendh_v.at[oe, peers[d]],
+            dst_ref=recvh_v.at[tp * n_ep + ep],
+            send_sem=h_ss,
+            recv_sem=h_rs,
+            device_id=(oe, peers[d]),
+            device_id_type=MESH,
+        ).start()
+    before_sub = iota((seqs, seqs), 1) < iota((seqs, seqs), 0)
+    ranks = []
+    for k in range(4):
+        same = jnp.zeros((seqs, seqs), F32)
+        for j in range(4):
+            same = same + (picks[k] == row4[j : j + 1, 0:seqs]).astype(F32)
+        same = jnp.where(before_sub, same, 0.0)
+        ranks.append(jnp.sum(same, axis=1, keepdims=True).astype(jnp.int32))
     rw = turned(rw_v[...])[0:seqs]
-    hots = [(e_lane == r).astype(F32) for r in picks]
-    named = hots[0] + hots[1] + hots[2] + hots[3]
-    earlier = (iota((seqs, seqs), 1) < iota((seqs, seqs), 0)).astype(BF16)
-    before = dot(earlier, named.astype(BF16))
-    ranks = [jnp.sum(h * before, axis=1, keepdims=True).astype(jnp.int32) for h in hots]
-    d_col = iota((seqs, n_ep * 8), 1)
-    pieces = []
-    for a in range(4):
-        piece = jnp.zeros((seqs, n_ep * 8), F32)
-        for k in range(4):
-            slot = (picks[k] // n_tp) * 8 + ranks[k] * 4 + a
-            slot = jnp.where(lax.rem(picks[k], n_tp) == tp, slot, -1)
-            piece = piece + (d_col == slot).astype(F32)
-        pieces.append(piece)
-    oh_v[...] = jnp.concatenate(pieces, axis=0).T.astype(BF16)
     m_col = iota((seqs, n_dev * 8), 1)
     for b in range(4):
         piece = jnp.zeros((seqs, n_dev * 8), F32)
@@ -371,7 +442,14 @@
     fold_v[0] = (i1 == lax.rem(i0, sq // 4) * 4 + i0 // (sq // 4)).astype(BF16)
     fold_v[1] = (i1 == lax.rem(i0, 4) * (sq // 4) + i0 // 4).astype(BF16)
 
-    copies[9].wait()
+    arrived = recv1_v.at[pl.ds(0, n_ep - 1)]
+    pltpu.make_async_copy(arrived, arrived, d_rs).wait()
+    n_rows = sq // 4
+    flat = dot(fold_v[0], recv1_v[...].reshape(sq, quarter)).astype(BF16)
+    for a in range(4):
+        tok_v[:, a * quarter : (a + 1) * quarter] = flat[a * n_rows : (a + 1) * n_rows]
+
+    copies["wo"].wait()
     share = heads * 64
 
     def project(owner):
@@ -383,35 +461,16 @@
         ho_copies[d].wait_recv()
         owner = lax.rem(tp + n_tp - d, n_tp)
         proj_v[...] += project(owner)
-    copies[8].wait()
     resid = (tokens_v[...].astype(F32) + proj_v[...]).astype(BF16)
-    quarter = width // n_tp
     for t in range(n_tp):
         resid_v[t] = resid[:, t * quarter : (t + 1) * quarter]
     rf = resid.astype(F32)
     mean = jnp.mean(rf * rf, axis=-1, keepdims=True)
     ffn_in = (rf * lax.rsqrt(mean + EPS) * ffn_gain_v[...]).astype(BF16)
 
-    folded = jnp.concatenate(
-        [ffn_in[:, a * quarter : (a + 1) * quarter] for a in range(4)], axis=0
-    )
-    packed = dot(oh_v[...], folded).astype(BF16)
-    send1_v[...] = packed.reshape(send1_v.shape)
-    recv1_v[ep] = send1_v[ep]
-
-    for other, _ in far_peers:
-        pltpu.make_async_remote_copy(
-            src_ref=send1_v.at[other],
-            dst_ref=recv1_v.at[ep],
-            send_sem=d_ss,
-            recv_sem=d_rs,
-            device_id=(other, tp),
-            device_id_type=MESH,
-        ).start()
-
-    copies[10].wait()
-    copies[11].wait()
-    copies[12].wait()
+    copies["wsg"].wait()
+    copies["wsu"].wait()
+    copies["wsd"].wait()
     gate = dot(ffn_in, wsg_v[...])
     up = dot(ffn_in, wsu_v[...])
     act = (gate / (1.0 + jnp.exp(-gate)) * up).astype(BF16)
@@ -432,14 +491,26 @@
         copy.start()
         sh_copies.append(copy)
 
-    copies[13].wait()
-    copies[14].wait()
-    copies[15].wait()
-    arrived = recv1_v.at[pl.ds(0, n_ep - 1)]
-    pltpu.make_async_copy(arrived, arrived, d_rs).wait()
-    flat = dot(fold_v[0], recv1_v[...].reshape(sq, quarter)).astype(BF16)
-    n_rows = sq // 4
-    lhs = jnp.concatenate([flat[a * n_rows : (a + 1) * n_rows] for a in range(4)], axis=1)
+    copies["wg"].wait()
+    copies["wu"].wait()
+    copies["wd"].wait()
+    heads_all = recvh_v.at[pl.ds(0, n_dev - 1)]
+    pltpu.make_async_copy(heads_all, heads_all, h_rs).wait()
+    gathered = jnp.concatenate(
+        [recvh_v[t * n_ep : (t + 1) * n_ep].reshape(sq, 128) for t in range(n_tp)], axis=1
+    )
+    flat = dot(fold_v[0, 0 : 2 * n_rows, :], gathered).astype(BF16)
+    total = jnp.zeros((n_rows, width), F32)
+    for t in range(n_tp):
+        lhs = jnp.concatenate(
+            [flat[a * n_rows : (a + 1) * n_rows, t * 128 : (t + 1) * 128] for a in range(2)],
+            axis=1,
+        )
+        part = dot(lhs, wo_v[t * share : (t + 1) * share, :])
+        total = total + part.astype(BF16).astype(F32)
+    rf = (tok_v[...].astype(F32) + total).astype(BF16).astype(F32)
+    mean = jnp.mean(rf * rf, axis=-1, keepdims=True)
+    lhs = (rf * lax.rsqrt(mean + EPS) * ffn_gain_v[...]).astype(BF16)
     gate = dot(lhs, wg_v[...])
     up = dot(lhs, wu_v[...])
     act = (gate / (1.0 + jnp.exp(-gate)) * up).astype(BF16)
@@ -462,8 +533,6 @@
         send2_v[:, t] = back[:, t * 128 : (t + 1) * 128].reshape(n_ep, 8, 128)
     recv2_v[me] = send2_v[ep, tp]
 
-    pl.semaphore_wait(relay_sem, n_tp - 1)
-
     def give(oe, ot):
         pltpu.make_async_remote_copy(
             src_ref=send2_v.at[oe, ot],
@@ -474,7 +543,7 @@
             device_id_type=MESH,
         ).start()
 
-    for _, oe, d in far_all:
+    for *_, d, oe in far_all:
         give(oe, peers[d])
 
     final = resid_v[tp].astype(F32) + shs_v[tp].astype(F32)
@@ -499,6 +568,7 @@
     sent = send1_v.at[pl.ds(0, n_ep - 1)]
     pltpu.make_async_copy(sent, sent, d_ss).wait()
     pltpu.make_async_copy(back_all, back_all, r_ss).wait()
+    pltpu.make_async_copy(heads_all, heads_all, h_ss).wait()
 
 
 def solution(mesh):
@@ -585,6 +655,11 @@
             pltpu.VMEM((seqs, width), F32),
             pltpu.VMEM((n_tp, seqs, quarter), BF16),
             pltpu.VMEM((n_ep * 8, 4 * seqs), BF16),
+            pltpu.VMEM((n_ep * 8, 8 * seqs), BF16),
+            pltpu.VMEM((8 * seqs, n_tp * 128), BF16),
+            pltpu.VMEM((n_ep, n_tp, 8, 128), BF16),
+            pltpu.VMEM((n_dev, 8, 128), BF16),
+            pltpu.VMEM((2 * n_ep, width), BF16),
             pltpu.VMEM((2, n_ep * 8, n_ep * 8), BF16),
             pltpu.VMEM((8 * seqs, n_dev * 8), BF16),
             pltpu.VMEM((n_ep, 8, quarter), BF16),
@@ -601,6 +676,8 @@
             pltpu.SemaphoreType.DMA,
             pltpu.SemaphoreType.DMA((n_tp,)),
             pltpu.SemaphoreType.DMA((n_tp,)),
+            pltpu.SemaphoreType.DMA,
+            pltpu.SemaphoreType.DMA,
             pltpu.SemaphoreType.DMA,
             pltpu.SemaphoreType.DMA,
             pltpu.SemaphoreType.REGULAR,

time: 32.8 us -> 31.8 us (0.970)
  Pallas kernels: 31.3 us -> 30.3 us
    pallas_call x1, Pallas kernels: 31.3 us -> 30.3 us  [shards(): pl.pallas_call(kernel, name='layer', out_shape=jax.ShapeDtypeStruct((seqs...]
where the time goes in v4:
time: 31.8 us; the launch traced here: 31.6 us
  Pallas kernels  30.3 us (95%)
  local copies, waits for them, and re-layouts  1.38 us (4%)
    pallas_call x1, Pallas kernels, shards(): pl.pallas_call(kernel, name='layer', out_shape=jax.ShapeDtypeStruct((seqs...  30.3 us
    unnamed x1, local copies, waits for them, and re-layouts  1.38 us

profile of v4, /device:TPU:1, one launch (start us, length us, event | category | flops | bytes accessed | tf_op | source)
XLA Modules:
  0.0 31.6 jit_solution(750556077915526328)
XLA Ops:
  0.0 30.3 %layer.1 = bf16[32,512]{1,0:T(8,128)(2,1)} custom-call(bf16[32,2048]{1,0:T(8,128)(2,1)} %refs_0_.1, bf16[32,1024,128]{2,1,0:T(8,128)(2,1)} %refs_1_.1, s32[32]{0:T(128)} %refs_2_.1, f32[1,2048]{1,0:T(1,128)} %bitcast.10, bf16[2048,256]{1,0:T(8,128)(2,1)} %refs_4_.1, bf16[64,2048]{1,0:T(8,128)(2,1)} %bitcast.7, bf16[64,2048]{1,0:T(8,128)(2,1)} %bitcast.8, ...), custom_call_target="tpu_custom_call" | custom-call | tf_op jit(solution)/shard_map/layer/pallas_call | solution.py:689
  30.3 1.4 %copy.21 = bf16[32,512]{1,0:T(8,128)(2,1)} copy(bf16[32,512]{1,0:T(8,128)(2,1)} %layer.1) | data formatting | bytes 65536
